TPU v7x, 512 devices: a whole 4x4x16 slice. The times are simulated.
512 devices in a mesh: rep: 2 (over z_hi), fs: 32 (over z_lo, y), tp: 8 (over x, core).
Axes of the slice: x: 4, y: 4, z: 16 (z_hi: 2, z_lo: 8; z = z_hi * 8 + z_lo), core: 2. Of those that a mesh axis runs over, the one named last changes fastest.
Arguments:
- inputs: bfloat16 [2, 12288, 2048], P('rep', 'fs', 'tp'), may hold values from -6 to 6
- gate_proj: bfloat16 [2048, 2816], P('fs', 'tp'), may hold values from -0.125 to 0.125
- value_proj: bfloat16 [2048, 2816], P('fs', 'tp'), may hold values from -0.125 to 0.125
- gate_taps: float32 [3, 2816], replicated, may hold values from -3 to 3
- value_taps: float32 [3, 2816], replicated, may hold values from -3 to 3
- out_grad: bfloat16 [2, 12288, 2816], P('rep', 'fs', 'tp'), may hold values from -6 to 6
Outputs:
- in_grad: bfloat16 [2, 12288, 2048], P('rep', 'fs', 'tp')
- gate_proj_grad: float32 [2048, 2816], P('fs', 'tp')
- value_proj_grad: float32 [2048, 2816], P('fs', 'tp')
- gate_taps_grad: float32 [3, 2816], replicated
- value_taps_grad: float32 [3, 2816], replicated
All inputs are finite; a program needn't handle non-finite values.
Results may differ from a plain program's by a relative error of at most 0.013.
Values may be sent and summed in bfloat16 or wider, within the bound.
A program may use at most 64 MiB of HBM per device.

v0:
```python
import jax
import jax.numpy as jnp
from jax import lax
from jax.sharding import Mesh
from jax.sharding import PartitionSpec as P

FS = ("fs_0", "fs_1")
REP_FS = ("rep", "fs_0", "fs_1")


def joined_along(blocks, dim):
    shape = list(blocks.shape[1:])
    shape[dim] *= blocks.shape[0]
    return jnp.moveaxis(blocks, 0, dim).reshape(shape)


def sent_to_all(shard, axis):
    copies = jnp.broadcast_to(shard, (lax.axis_size(axis), *shard.shape))
    return lax.all_to_all(copies, axis, split_axis=0, concat_axis=0, tiled=True)


def gather_directly(shard, axis, dim):
    return joined_along(sent_to_all(shard, axis), dim)


def stacked_from(shard, axes, turns):
    blocks = shard
    for k in turns:
        blocks = lax.all_gather(blocks, axes[k])
    done = turns[::-1]
    back = [done.index(k) for k in range(len(axes))]
    blocks = blocks.transpose(*back, *range(len(axes), blocks.ndim))
    return blocks.reshape(-1, *shard.shape)


def gather_axes(shard, axes, turns, dim):
    return joined_along(stacked_from(shard, axes, turns), dim)


def with_halo(cells, sides, width):
    for axis, dim in sides:
        count = lax.axis_size(axis)
        ends = count - 1
        head = lax.slice_in_dim(cells, 0, width, axis=dim)
        tail = lax.slice_in_dim(cells, cells.shape[dim] - width, cells.shape[dim], axis=dim)
        cells = jnp.concatenate(
            [
                lax.ppermute(tail, axis, [(i, (i + 1) % count) for i in range(ends)]),
                cells,
                lax.ppermute(head, axis, [((i + 1) % count, i) for i in range(ends)]),
            ],
            axis=dim,
        )
    return cells


def split_up(shard, dim, peers):
    before, after = (shard.shape[:dim], shard.shape[dim + 1 :])
    return jnp.moveaxis(shard.reshape(*before, peers, -1, *after), dim, 0)


def sent_and_summed(shard, axis, dim):
    peers = lax.axis_size(axis)
    blocks = lax.all_to_all(split_up(shard, dim, peers), axis, 0, 0, tiled=True)
    return jnp.sum(blocks.astype(jnp.float32), axis=0)


def over_copies(shard, axis):
    return sent_to_all(shard, axis).sum(axis=0)


def mix_taps(pre_wide, taps_both, count):
    return (
        taps_both[:, 0, None, :] * pre_wide[:, 0:count]
        + taps_both[:, 1, None, :] * pre_wide[:, 1 : count + 1]
        + taps_both[:, 2, None, :] * pre_wide[:, 2 : count + 2]
    )


def back_taps(cot_wide, taps_both, count):
    return (
        taps_both[:, 0, None, :] * cot_wide[:, 2 : count + 2]
        + taps_both[:, 1, None, :] * cot_wide[:, 1 : count + 1]
        + taps_both[:, 2, None, :] * cot_wide[:, 0:count]
    )


def cotangents(gate_mix, value_mix, cot_in):
    sigmoid_gate = jax.nn.sigmoid(gate_mix)
    gate_cot = cot_in * value_mix * (sigmoid_gate * (1.0 + gate_mix * (1.0 - sigmoid_gate)))
    value_cot = cot_in * (gate_mix * sigmoid_gate)
    return (gate_cot, value_cot)


def shards(inputs, gate_proj, value_proj, gate_taps, value_taps, out_grad):
    contract_cols = (((1,), (1,)), ((), ()))
    contract_rows = (((0,), (0,)), ((), ()))
    tok_rows = inputs.shape[1]
    hid_cols = gate_proj.shape[1]
    gathered = gather_directly(inputs, "tp", 2)[0]
    col_start = lax.axis_index("tp") * hid_cols
    taps_both = jnp.stack(
        [
            lax.dynamic_slice_in_dim(gate_taps, col_start, hid_cols, 1),
            lax.dynamic_slice_in_dim(value_taps, col_start, hid_cols, 1),
        ]
    )
    stacked = jnp.stack([gate_proj, value_proj])
    full_rows = gather_axes(stacked, FS, (0, 1), 1)
    gate_acc = jnp.dot(gathered, full_rows[0], preferred_element_type=jnp.float32)
    value_acc = jnp.dot(gathered, full_rows[1], preferred_element_type=jnp.float32)
    pre_acts = jnp.stack([gate_acc, value_acc]).astype(jnp.bfloat16)
    deep_wide = with_halo(jnp.concatenate([pre_acts, out_grad], axis=0), ((FS, 1),), 2).astype(
        jnp.float32
    )
    mix_out = mix_taps(deep_wide[:2], taps_both, tok_rows + 2)
    gate_cot, value_cot = cotangents(mix_out[0], mix_out[1], deep_wide[2, 1 : tok_rows + 3])
    cot_wide = jnp.stack([gate_cot, value_cot])
    cot_rows = cot_wide[:, 1 : tok_rows + 1]
    pre_wide = deep_wide[:2, 1 : tok_rows + 3]
    pre_cot = back_taps(cot_wide, taps_both, tok_rows).astype(jnp.bfloat16)
    tap_terms = jnp.stack(
        [
            jnp.sum(pre_wide[:, offset : offset + tok_rows] * cot_rows, axis=1)
            for offset in range(3)
        ],
        axis=1,
    )
    partial_value = lax.dot_general(
        pre_cot[0], full_rows[0], contract_cols, preferred_element_type=jnp.float32
    ) + lax.dot_general(pre_cot[1], full_rows[1], contract_cols, preferred_element_type=jnp.float32)
    in_grad = sent_and_summed(partial_value.astype(jnp.bfloat16), "tp", 1).astype(jnp.bfloat16)[
        None
    ]
    grad_terms = jnp.stack(
        [
            lax.dot_general(
                gathered, pre_cot[0], contract_rows, preferred_element_type=jnp.float32
            ),
            lax.dot_general(
                gathered, pre_cot[1], contract_rows, preferred_element_type=jnp.float32
            ),
        ]
    )
    received = lax.all_to_all(
        grad_terms.astype(jnp.bfloat16), FS, split_axis=1, concat_axis=0, tiled=True
    ).astype(grad_terms.dtype)
    fs_count = lax.axis_size(FS)
    own_sum = jnp.sum(received.reshape(fs_count, 2, received.shape[1], hid_cols), axis=0)
    own_sum = over_copies(own_sum, "rep")
    taps_total = over_copies(tap_terms, REP_FS)
    taps_all = gather_directly(taps_total, "tp", 2)
    factor = float(tok_rows * fs_count * lax.axis_size("rep")) ** (-0.5)
    return (
        in_grad,
        own_sum[0] * factor,
        own_sum[1] * factor,
        taps_all[0] * factor,
        taps_all[1] * factor,
    )


def solution(mesh):
    torus = Mesh(
        mesh.devices.reshape(mesh.shape["rep"], 8, 4, mesh.shape["tp"]),
        ("rep", "fs_0", "fs_1", "tp"),
    )
    placed = (P("rep", FS, "tp"), P(FS, "tp"), P(FS, "tp"), P(), P(), P("rep", FS, "tp"))
    return jax.shard_map(
        shards,
        mesh=torus,
        in_specs=placed,
        out_specs=(P("rep", FS, "tp"), P(FS, "tp"), P(FS, "tp"), P(), P()),
        check_vma=False,
    )
```

profile of v0, /device:TPU:32, one launch (start us, length us, event | category | flops | bytes accessed | tf_op | source)
XLA Modules:
  0.0 406.3 jit_solution(9321597463978439638)
XLA Ops:
  8.1 53.7 %all-gather = bf16[16,64,352]{2,1,0:T(8,128)(2,1)} all-gather(bf16[2,64,352]{2,1,0:T(8,128)(2,1)S(1)} %pad_maximum_fusion.5), channel_id=2, replica_groups=mesh['rep'=2,'fs_0'=8,'fs_1'=4,'tp'=8] {'fs_0'}, dimensions={0}, use_global_device_ids=true | all-gather | bytes 811008 | tf_op jit(solution)/shard_map/all_gather | solution.py:29
  63.3 4.2 %all-to-all-start = ((bf16[8,1,384,256]{2,3,1,0:T(8,128)(2,1)}), bf16[8,1,384,256]{2,3,1,0:T(8,128)(2,1)S(1)}, u32[]{:S(2)}, u32[]{:S(2)}) async-start(bf16[8,1,384,256]{2,3,1,0:T(8,128)(2,1)} %broadcast_in_dim.15), calls=%async_computation | async-start | bytes 3145728 | tf_op jit(solution)/shard_map/all_to_all | solution.py:19
  68.3 42.5 %all-gather.4.cloned.1.call-done = bf16[32,2,64,352]{3,2,1,0:T(8,128)(2,1)} async-done(((bf16[8,2,64,352]{3,2,1,0:T(8,128)(2,1)}), bf16[32,2,64,352]{3,2,1,0:T(8,128)(2,1)}) %all-gather.4.cloned.1.call-update) | async-done | bytes 2883600 | tf_op jit(solution)/shard_map/all_gather | solution.py:29
  110.9 2.4 copy.49
  114.8 2.3 fusion.5
  118.3 2.6 collective-permute-start.1
  121.0 3.2 collective-permute-start
  124.2 4.1 %collective-permute-done.1 = bf16[3,2,352]{1,2,0:T(8,128)(2,1)S(1)} collective-permute-done((bf16[3,2,352]{1,2,0:T(8,128)(2,1)S(1)}, bf16[3,2,352]{1,2,0:T(8,128)(2,1)S(1)}, u32[]{:S(2)}, u32[]{:S(2)}) %collective-permute-start.1) | collective-permute-done | bytes 4256 | tf_op jit(solution)/shard_map/ppermute | solution.py:50
  128.3 4.5 %collective-permute-done = bf16[3,2,352]{1,2,0:T(8,128)(2,1)S(1)} collective-permute-done((bf16[3,2,352]{1,2,0:T(8,128)(2,1)S(1)}, bf16[3,2,352]{1,2,0:T(8,128)(2,1)S(1)}, u32[]{:S(2)}, u32[]{:S(2)}) %collective-permute-start) | collective-permute-done | bytes 4256 | tf_op jit(solution)/shard_map/ppermute | solution.py:48
  135.0 2.3 fusion.14
  138.3 13.6 %all-to-all-start.4 = ((f32[64,2,3,352]{3,1,2,0:T(2,128)}), f32[64,2,3,352]{3,1,2,0:T(2,128)}, u32[]{:S(2)}, u32[]{:S(2)}) async-start(f32[64,2,3,352]{3,1,2,0:T(2,128)} %broadcast_in_dim.18), calls=%async_computation.4 | async-start | bytes 1179648 | tf_op jit(solution)/shard_map/all_to_all | solution.py:19
  151.9 2.7 fusion.11
  158.4 8.7 %copy.53 = bf16[2,2048,352]{2,0,1:T(2,128)(2,1)} copy(bf16[2,2048,352]{1,2,0:T(8,128)(2,1)} %pad_maximum_fusion) | data formatting | bytes 5767168 | tf_op jit(solution)/shard_map/stack | solution.py:135
  167.1 17.9 %all-to-all-done.4 = f32[64,2,3,352]{3,1,2,0:T(2,128)} async-done(((f32[64,2,3,352]{3,1,2,0:T(2,128)}), f32[64,2,3,352]{3,1,2,0:T(2,128)}, u32[]{:S(2)}, u32[]{:S(2)}) %all-to-all-start.4) | async-done | bytes 540704 | tf_op jit(solution)/shard_map/all_to_all | solution.py:19
  185.0 6.4 %all-to-all-start.2 = ((bf16[2,2048,352]{2,0,1:T(2,128)(2,1)}), bf16[2,2048,352]{2,0,1:T(2,128)(2,1)}, u32[]{:S(2)}, u32[]{:S(2)}) async-start(bf16[2,2048,352]{2,0,1:T(2,128)(2,1)} %copy.53), calls=%async_computation.2 | async-start | bytes 6291456 | tf_op jit(solution)/shard_map/all_to_all | solution.py:145
  195.1 133.1 %all-to-all-done.2 = bf16[2,2048,352]{2,0,1:T(2,128)(2,1)} async-done(((bf16[2,2048,352]{2,0,1:T(2,128)(2,1)}), bf16[2,2048,352]{2,0,1:T(2,128)(2,1)}, u32[]{:S(2)}, u32[]{:S(2)}) %all-to-all-start.2) | async-done | bytes 2883616 | tf_op jit(solution)/shard_map/all_to_all | solution.py:145
  328.2 4.3 %all-to-all-start.1 = ((bf16[8,384,256]{2,1,0:T(8,128)(2,1)}), bf16[8,384,256]{2,1,0:T(8,128)(2,1)}, u32[]{:S(2)}, u32[]{:S(2)}) async-start(bf16[8,384,256]{2,1,0:T(8,128)(2,1)} %bitcast.77), calls=%async_computation.1 | async-start | bytes 3145728 | tf_op jit(solution)/shard_map/all_to_all | solution.py:64
  333.8 2.3 copy.54
  336.1 18.0 %all-to-all-done.1 = bf16[8,384,256]{2,1,0:T(8,128)(2,1)} async-done(((bf16[8,384,256]{2,1,0:T(8,128)(2,1)}), bf16[8,384,256]{2,1,0:T(8,128)(2,1)}, u32[]{:S(2)}, u32[]{:S(2)}) %all-to-all-start.1) | async-done | bytes 1572896 | tf_op jit(solution)/shard_map/all_to_all | solution.py:64
  354.8 3.4 all-to-all-start.5
  358.7 5.0 %all-to-all-done.5 = f32[8,2,3,352]{3,1,2,0:T(2,128)S(1)} async-done(((f32[8,2,3,352]{3,1,2,0:T(2,128)}), f32[8,2,3,352]{3,1,2,0:T(2,128)S(1)}, u32[]{:S(2)}, u32[]{:S(2)}) %all-to-all-start.5) | async-done | bytes 67616 | tf_op jit(solution)/shard_map/all_to_all | solution.py:19
  364.5 6.5 %all-to-all-start.3 = ((f32[2,2,64,352]{3,2,1,0:T(8,128)}), f32[2,2,64,352]{3,2,1,0:T(8,128)S(1)}, u32[]{:S(2)}, u32[]{:S(2)}) async-start(f32[2,2,64,352]{3,2,1,0:T(8,128)} %broadcast_in_dim.17), calls=%async_computation.3 | async-start | bytes 786432 | tf_op jit(solution)/shard_map/all_to_all | solution.py:19
  371.0 2.3 reduce_sum.66
  374.7 24.0 %all-to-all-done.3 = f32[2,2,64,352]{3,2,1,0:T(8,128)S(1)} async-done(((f32[2,2,64,352]{3,2,1,0:T(8,128)}), f32[2,2,64,352]{3,2,1,0:T(8,128)S(1)}, u32[]{:S(2)}, u32[]{:S(2)}) %all-to-all-start.3) | async-done | bytes 360480 | tf_op jit(solution)/shard_map/all_to_all | solution.py:19
  (48 shorter events, 22.0 us)
Async XLA Ops:
  7.2 54.7 %copy-start.6 = (bf16[1,384,256]{2,1,0:T(8,128)(2,1)S(1)}, bf16[1,384,256]{2,1,0:T(8,128)(2,1)}, u32[]{:S(2)}) copy-start(bf16[1,384,256]{2,1,0:T(8,128)(2,1)} %param.6) | copy-start | bytes 589828
  7.2 103.7 %all-gather.4.cloned.1.call-start = ((), (), s32[]{:S(2)}) async-start(), calls=%async_computation.6 | async-start | bytes 3932160 | tf_op jit(solution)/shard_map/all_gather | solution.py:29
  63.3 51.5 %all-to-all-start = ((bf16[8,1,384,256]{2,3,1,0:T(8,128)(2,1)}), bf16[8,1,384,256]{2,3,1,0:T(8,128)(2,1)S(1)}, u32[]{:S(2)}, u32[]{:S(2)}) async-start(bf16[8,1,384,256]{2,3,1,0:T(8,128)(2,1)} %broadcast_in_dim.15), calls=%async_computation | async-start | bytes 3145728 | tf_op jit(solution)/shard_map/all_to_all | solution.py:19
  117.2 1.0 copy-start.5
  118.3 9.9 %collective-permute-start.1 = (bf16[3,2,352]{1,2,0:T(8,128)(2,1)S(1)}, bf16[3,2,352]{1,2,0:T(8,128)(2,1)S(1)}, u32[]{:S(2)}, u32[]{:S(2)}) collective-permute-start(bf16[3,2,352]{1,2,0:T(8,128)(2,1)S(1)} %get-tuple-element.14), channel_id=1, source_target_pairs={{8,0},{16,8},{24,16},{32,24},{40,32},{48,40},{56,48},{64,56},{72,6... | collective-permute-start | bytes 12680 | tf_op jit(solution)/shard_map/ppermute | solution.py:50
  121.0 11.8 %collective-permute-start = (bf16[3,2,352]{1,2,0:T(8,128)(2,1)S(1)}, bf16[3,2,352]{1,2,0:T(8,128)(2,1)S(1)}, u32[]{:S(2)}, u32[]{:S(2)}) collective-permute-start(bf16[3,2,352]{1,2,0:T(8,128)(2,1)S(1)} %get-tuple-element.13), channel_id=1, source_target_pairs={{0,8},{8,16},{16,24},{24,32},{32,40},{40,48},{48,56},{56,64},{64,7... | collective-permute-start | bytes 12680 | tf_op jit(solution)/shard_map/ppermute | solution.py:48
  135.0 2.3 copy-start.1
  135.0 2.3 copy-start.2
  138.3 46.7 %all-to-all-start.4 = ((f32[64,2,3,352]{3,1,2,0:T(2,128)}), f32[64,2,3,352]{3,1,2,0:T(2,128)}, u32[]{:S(2)}, u32[]{:S(2)}) async-start(f32[64,2,3,352]{3,1,2,0:T(2,128)} %broadcast_in_dim.18), calls=%async_computation.4 | async-start | bytes 1179648 | tf_op jit(solution)/shard_map/all_to_all | solution.py:19
  154.6 1.0 copy-start.3
  167.1 24.3 %copy-start.4 = (bf16[2,384,352]{1,2,0:T(8,128)(2,1)S(1)}, bf16[2,384,352]{1,2,0:T(8,128)(2,1)}, u32[]{:S(2)}) copy-start(bf16[2,384,352]{1,2,0:T(8,128)(2,1)} %copy-done.3) | copy-start | bytes 1622020
  185.0 143.2 %all-to-all-start.2 = ((bf16[2,2048,352]{2,0,1:T(2,128)(2,1)}), bf16[2,2048,352]{2,0,1:T(2,128)(2,1)}, u32[]{:S(2)}, u32[]{:S(2)}) async-start(bf16[2,2048,352]{2,0,1:T(2,128)(2,1)} %copy.53), calls=%async_computation.2 | async-start | bytes 6291456 | tf_op jit(solution)/shard_map/all_to_all | solution.py:145
  191.4 1.4 copy-start
  328.2 25.9 %all-to-all-start.1 = ((bf16[8,384,256]{2,1,0:T(8,128)(2,1)}), bf16[8,384,256]{2,1,0:T(8,128)(2,1)}, u32[]{:S(2)}, u32[]{:S(2)}) async-start(bf16[8,384,256]{2,1,0:T(8,128)(2,1)} %bitcast.77), calls=%async_computation.1 | async-start | bytes 3145728 | tf_op jit(solution)/shard_map/all_to_all | solution.py:64
  354.8 8.9 %all-to-all-start.5 = ((f32[8,2,3,352]{3,1,2,0:T(2,128)}), f32[8,2,3,352]{3,1,2,0:T(2,128)S(1)}, u32[]{:S(2)}, u32[]{:S(2)}) async-start(f32[8,2,3,352]{3,1,2,0:T(2,128)} %broadcast_in_dim.19), calls=%async_computation.5 | async-start | bytes 147456 | tf_op jit(solution)/shard_map/all_to_all | solution.py:19
  364.5 34.2 %all-to-all-start.3 = ((f32[2,2,64,352]{3,2,1,0:T(8,128)}), f32[2,2,64,352]{3,2,1,0:T(8,128)S(1)}, u32[]{:S(2)}, u32[]{:S(2)}) async-start(f32[2,2,64,352]{3,2,1,0:T(8,128)} %broadcast_in_dim.17), calls=%async_computation.3 | async-start | bytes 786432 | tf_op jit(solution)/shard_map/all_to_all | solution.py:19
Sparse Core Ops, SparseCore 0:
  62.0 48.8 all-gather.3
where the time goes:
time: 407 us; the launch traced here: 406 us
  waiting for transfers between devices  249 us (61%)
  blocking collectives  53.7 us (13%)
  starting transfers between devices  44.2 us (11%)
  local copies, waits for them, and re-layouts  22.7 us (6%)
  other arithmetic  15 us (4%)
  between operations  14.3 us (4%)
  matrix products  7.26 us (2%)
    all_to_all x1, waiting for transfers between devices, shards(): lax.all_to_all(grad_terms.astype(jnp.bfloat16), FS, split_axis=1, concat_...  133 us
    all_gather x1, blocking collectives, stacked_from(): blocks = lax.all_gather(blocks, axes[k])  53.7 us
    all_to_all x4, waiting for transfers between devices, sent_to_all(): return lax.all_to_all(copies, axis, split_axis=0, concat_axis=0, tiled=True)  46.9 us
    all_gather x1, waiting for transfers between devices, stacked_from(): blocks = lax.all_gather(blocks, axes[k])  42.5 us
    all_to_all x4, starting transfers between devices, sent_to_all(): return lax.all_to_all(copies, axis, split_axis=0, concat_axis=0, tiled=True)  27.6 us
    all_to_all x1, waiting for transfers between devices, sent_and_summed(): blocks = lax.all_to_all(split_up(shard, dim, peers), axis, 0, 0, tiled=True)  18 us
    another operation x1, local copies, waits for them, and re-layouts, shards(): jnp.stack([lax.dot_general(gathered, pre_cot[0], contract_rows, preferred...  8.71 us
  transfers between devices with their start and end apart: 9, of which 8 were waited for; matrix products, arithmetic and copies ran while one was open for 8% of the time, Pallas kernels for 0%

commit v1 on v0

v1 whole, which is shorter than its diff:
```python
import functools

import jax
import jax.numpy as jnp
from jax import lax
from jax.experimental import pallas as pl
from jax.experimental.pallas import tpu as pltpu
from jax.sharding import PartitionSpec as P

MESH = pl.DeviceIdType.MESH
BF16 = jnp.bfloat16
F32 = jnp.float32

NX, NC, NY, NZ = 4, 2, 4, 16
ZL = 8
TOK = 384
COLS = 352
FEAT = 256
EDGE = 16
EXT = TOK + 2 * EDGE


def right_reach(r):
    return 4 if r < 2 else 3


class Wires:
    def __init__(self, send_sems, recv_sems):
        self.send_sems, self.recv_sems = send_sems, recv_sems
        self.index = {}
        self.sent = []

    def at(self, key):
        return self.index.setdefault(key, len(self.index))

    def send(self, key, src, dst, to):
        i = self.at(key)
        copy = pltpu.make_async_remote_copy(
            src_ref=src,
            dst_ref=dst,
            send_sem=self.send_sems.at[i],
            recv_sem=self.recv_sems.at[i],
            device_id=to,
            device_id_type=MESH,
        )
        copy.start()
        self.sent.append(copy)

    def wait(self, key, dst, to):
        i = self.at(key)
        pltpu.make_async_remote_copy(
            src_ref=dst,
            dst_ref=dst,
            send_sem=self.send_sems.at[i],
            recv_sem=self.recv_sems.at[i],
            device_id=to,
            device_id_type=MESH,
        ).wait_recv()

    def drain(self):
        for copy in self.sent:
            copy.wait_send()


def kernel(
    factor,
    x_hbm, wg_hbm, wv_hbm, ogt_hbm, taps_ref,
    din_ref, dg_ref, dv_ref, tout_ref,
    X, WG, WV, OGT, OG, PG, PV, KG, KV, CG, CV, GG, GV,
    FARG, FARV, DIRG, DIRV, MIDG, MIDV, ENDG, ENDV, RG, RV,
    ZRG, ZLG, ZRV, ZLV, TRG, TLG, TRV, TLV,
    IP, IR, IS, ISR, TY, TZ1, TB, TT,
    send_sems, recv_sems, local_sems,
):
    rep, fs, tp = lax.axis_index("rep"), lax.axis_index("fs"), lax.axis_index("tp")
    zl, y = lax.div(fs, NY), lax.rem(fs, NY)
    x, c = lax.div(tp, NC), lax.rem(tp, NC)
    zg = rep * ZL + zl

    def dev(x=x, c=c, y=y, z=zg):
        z = lax.rem(z + NZ, NZ)
        return (
            lax.div(z, ZL),
            lax.rem(z, ZL) * NY + lax.rem(y + NY, NY),
            lax.rem(x + NX, NX) * NC + c,
        )

    def blk(dz, dy):
        return lax.rem(zl + dz + ZL, ZL) * NY + lax.rem(y + dy + NY, NY)

    def zrow(dz):
        return lax.rem(zl + dz + 2 * ZL, ZL)

    me = dev()
    right, left = dev(z=zg + 1), dev(z=zg - 1)
    up, down = dev(y=y + 1), dev(y=y - 1)
    partner = dev(c=1 - c)
    after_z = zg + lax.div(y + 1, NY)
    after = dev(y=y + 1, z=after_z)
    before_z = zg - 1 + lax.div(y + NY - 1, NY)
    before = dev(y=y - 1, z=before_z)

    def tp_peer(k):
        return (rep, fs, lax.rem(tp + k + 8, 8))

    zq, zo = lax.div(zg, 4), lax.rem(zg, 4)
    side = 4 * (1 - 2 * lax.rem(zq, 2))

    def z_near(k):
        return dev(z=zq * 4 + lax.rem(zo + k, 4))

    own = blk(0, 0)
    loads = [
        pltpu.make_async_copy(wg_hbm, WG.at[own], local_sems.at[0]),
        pltpu.make_async_copy(wv_hbm, WV.at[own], local_sems.at[1]),
        pltpu.make_async_copy(x_hbm, X.at[tp, pl.ds(EDGE, TOK)], local_sems.at[2]),
        pltpu.make_async_copy(ogt_hbm, OGT.at[pl.ds(0, COLS)], local_sems.at[3]),
    ]
    for load in loads:
        load.start()

    barrier = pltpu.get_barrier_semaphore()
    peers = [tp_peer(k) for k in range(1, 8)]
    peers += [dev(y=y + k) for k in (1, 2, 3)]
    peers += [right, left, after, before]
    peers += [z_near(k) for k in (1, 2, 3)]
    peers += [dev(z=zg + 4), dev(z=zg - 4)]
    for peer in peers:
        pl.semaphore_signal(barrier, inc=1, device_id=peer, device_id_type=MESH)
    pl.semaphore_wait(barrier, len(peers))

    w = Wires(send_sems, recv_sems)

    loads[0].wait()
    for dy in (1, 3, 2):
        w.send(("gy", dy), WG.at[own], WG.at[own], dev(y=y + dy))
    loads[1].wait()
    w.send(("vz", 1, 1), WV.at[own], WV.at[own], right)
    w.send(("vz", -1, 1), WV.at[own], WV.at[own], left)
    w.send(("gz", 0, 1, 1), WG.at[own], WG.at[own], right)
    w.send(("gz", 0, -1, 1), WG.at[own], WG.at[own], left)
    loads[2].wait()
    mine = X.at[tp, pl.ds(EDGE, TOK)]
    for dx in (1, 3, 2):
        w.send(("x", dx), mine, mine, dev(x=x + dx))
    w.send(("xp", 0), mine, mine, partner)
    head, tail = X.at[tp, pl.ds(EDGE, EDGE)], X.at[tp, pl.ds(TOK, EDGE)]
    lo, hi = pl.ds(0, EDGE), pl.ds(TOK + EDGE, EDGE)
    w.send(("hx", 1), tail, X.at[tp, lo], after)
    w.send(("hx", -1), head, X.at[tp, hi], before)
    w.send(("vy", 0, 1), WV.at[own], WV.at[own], up)
    w.send(("vy", 0, -1), WV.at[own], WV.at[own], down)

    for r in (3, 1, 2):
        unit = WG.at[blk(0, r)]
        w.wait(("gy", 4 - r), unit, me)
        w.send(("gz", r, 1, 1), unit, unit, right)
        w.send(("gz", r, -1, 1), unit, unit, left)

    def out_grad_rows():
        loads[3].wait()
        for i in range(3):
            for j in range(3):
                block = OGT[128 * i : 128 * i + 128, 128 * j : 128 * j + 128].astype(F32)
                cols = min(128, COLS - 128 * i)
                OG[EDGE + 128 * j : EDGE + 128 * j + 128, 128 * i : 128 * i + cols] = (
                    block.T[:, :cols].astype(BF16)
                )

    def gate_chunk(z, first=False):
        part = jnp.dot(
            X[z],
            WG[pl.ds(z * NY, NY)].reshape(FEAT, COLS),
            preferred_element_type=F32,
        )
        if first:
            PG[8 : 8 + EXT] = part
        else:
            PG[8 : 8 + EXT] += part

    def value_chunk(z, first=False):
        part = jnp.dot(
            X[z],
            WV[pl.ds(z * NY, NY)].reshape(FEAT, COLS),
            preferred_element_type=F32,
        )
        if first:
            PV[8 : 8 + EXT] = part
        else:
            PV[8 : 8 + EXT] += part

    def x_arrived(dx):
        slot = X.at[lax.rem(x - dx + NX, NX) * NC + c, pl.ds(EDGE, TOK)]
        w.wait(("x", dx), slot, me)
        w.send(("xp", dx), slot, slot, partner)

    def xp_arrived(dx):
        slot = X.at[lax.rem(x - dx + NX, NX) * NC + 1 - c, pl.ds(EDGE, TOK)]
        w.wait(("xp", dx), slot, me)

    def value_row_sent(dz):
        unit = WV.at[blk(dz, 0)]
        w.send(("vy", dz, 1), unit, unit, up)
        w.send(("vy", dz, -1), unit, unit, down)

    def value_row_arrived(dz):
        from_down, from_up = WV.at[blk(dz, -1)], WV.at[blk(dz, 1)]
        w.wait(("vy", dz, 1), from_down, me)
        if dz % 2 == 0:
            w.send(("vf", dz), from_down, from_down, up)
        w.wait(("vy", dz, -1), from_up, me)
        if dz % 2 == 1:
            w.send(("vf", dz), from_up, from_up, down)

    def value_row_done(dz):
        w.wait(("vf", dz), WV.at[blk(dz, 2)], me)

    rows_sent = [[0]]
    for d in range(1, 5):
        sent = []
        for way, reach, to in ((1, 4, right), (-1, 3, left)):
            if d <= reach:
                unit = WV.at[blk(-way * d, 0)]
                w.wait(("vz", way, d), unit, me)
                if d < reach:
                    w.send(("vz", way, d + 1), unit, unit, to)
                value_row_sent(-way * d)
                sent.append(-way * d)
        for r in (0, 3, 1, 2):
            for way, reach, to in ((1, right_reach(r), right), (-1, 7 - right_reach(r), left)):
                if d <= reach:
                    unit = WG.at[blk(-way * d, r)]
                    w.wait(("gz", r, way, d), unit, me)
                    if d < reach:
                        w.send(("gz", r, way, d + 1), unit, unit, to)
        for dz in rows_sent[-1]:
            value_row_arrived(dz)
        rows_sent.append(sent)
        if d == 1:
            w.wait(("hx", 1), X.at[tp, lo], me)
            w.wait(("hx", -1), X.at[tp, hi], me)
            for k in range(1, 8):
                w.send(("hl", k), X.at[tp, lo], X.at[tp, lo], tp_peer(k))
                w.send(("hr", k), X.at[tp, hi], X.at[tp, hi], tp_peer(k))
            x_arrived(1)
            x_arrived(3)
            out_grad_rows()
        if d == 2:
            w.send(("og", 1), OG.at[pl.ds(TOK, EDGE)], OG.at[lo], after)
            w.send(("og", -1), OG.at[pl.ds(EDGE, EDGE)], OG.at[hi], before)
            x_arrived(2)
            for dx in (0, 1, 3, 2):
                xp_arrived(dx)
            for k in range(1, 8):
                t = lax.rem(tp - k + 8, 8)
                w.wait(("hl", k), X.at[t, lo], me)
                w.wait(("hr", k), X.at[t, hi], me)
            gate_chunk(zrow(0), first=True)
            gate_chunk(zrow(1))
            gate_chunk(zrow(-1))
        if d == 3:
            gate_chunk(zrow(2))
            gate_chunk(zrow(-2))
            for dz in rows_sent[0] + rows_sent[1]:
                value_row_done(dz)
            value_chunk(zrow(0), first=True)
            value_chunk(zrow(1))
            value_chunk(zrow(-1))
    for dz in rows_sent[-1]:
        value_row_arrived(dz)
    gate_chunk(zrow(3))
    gate_chunk(zrow(-3))
    gate_chunk(zrow(4))
    for dz in rows_sent[2] + rows_sent[3] + rows_sent[4]:
        value_row_done(dz)
        value_chunk(zrow(dz))
    w.wait(("og", 1), OG.at[lo], me)
    w.wait(("og", -1), OG.at[hi], me)

    not_first, not_last = fs > 0, fs < NY * ZL - 1
    for ref in (PG, PV):
        ref[8 : 8 + EDGE] = jnp.where(not_first, ref[8 : 8 + EDGE], 0.0)
        ref[8 + EDGE + TOK : 8 + EXT] = jnp.where(not_last, ref[8 + EDGE + TOK : 8 + EXT], 0.0)
    OG[:EDGE] = jnp.where(not_first, OG[:EDGE].astype(F32), 0.0).astype(BF16)
    OG[EDGE + TOK :] = jnp.where(not_last, OG[EDGE + TOK :].astype(F32), 0.0).astype(BF16)

    g0, g1, g2 = (taps_ref[0, k : k + 1, :] for k in range(3))
    v0, v1, v2 = (taps_ref[1, k : k + 1, :] for k in range(3))

    def rounded(value):
        return value.astype(BF16).astype(F32)

    def cot_rows(i):
        base = pl.multiple_of(i * 16, 16)
        gate = rounded(PG[pl.ds(base, 32)])
        value = rounded(PV[pl.ds(base, 32)])
        gm, gz, gp = gate[7:23], gate[8:24], gate[9:25]
        vm, vz, vp = value[7:23], value[8:24], value[9:25]
        gate_mix = g0 * gm + g1 * gz + g2 * gp
        value_mix = v0 * vm + v1 * vz + v2 * vp
        grad = OG[pl.ds(base, 16)].astype(F32)
        s = jax.nn.sigmoid(gate_mix)
        gate_cot = grad * value_mix * (s * (1.0 + gate_mix * (1.0 - s)))
        value_cot = grad * (gate_mix * s)
        KG[pl.ds(base + 8, 16)] = gate_cot
        KV[pl.ds(base + 8, 16)] = value_cot
        return [
            (p * k).reshape(2, 8, COLS).sum(axis=0)
            for p, k in (
                (gm, gate_cot), (gz, gate_cot), (gp, gate_cot),
                (vm, value_cot), (vz, value_cot), (vp, value_cot),
            )
        ]

    cot_rows(0)
    cot_rows(TOK // 16 + 1)
    zero = jnp.zeros((8, COLS), F32)
    tap_sums = lax.fori_loop(
        1, TOK // 16 + 1,
        lambda i, sums: tuple(a + b for a, b in zip(sums, cot_rows(i))),
        (zero,) * 6,
    )

    def back_rows(i, carry):
        base = pl.multiple_of(i * 16, 16)
        out = pl.ds(pl.multiple_of(i * 16 - 16, 16), 16)
        for source, target, (t0, t1, t2) in ((KG, CG, (g0, g1, g2)), (KV, CV, (v0, v1, v2))):
            cot = source[pl.ds(base, 32)]
            target[out] = (t0 * cot[9:25] + t1 * cot[8:24] + t2 * cot[7:23]).astype(BF16)
        return carry

    lax.fori_loop(1, TOK // 16 + 1, back_rows, 0)

    rows = [jnp.sum(part, axis=0, keepdims=True) for part in tap_sums]
    TY[y] = jnp.concatenate(rows + [jnp.zeros((2, COLS), F32)], axis=0)

    order = (0, 1, -1, 2, -2, 3, -3, 4)
    place = {dz % ZL: k for k, dz in enumerate(order)}

    def make_blocks(k):
        z = zrow(order[k])
        acts = X[z, EDGE : EDGE + TOK, :]
        for cot, terms in ((CG, GG), (CV, GV)):
            block = lax.dot_general(
                acts, cot[...], (((0,), (0,)), ((), ())), preferred_element_type=F32
            )
            terms[pl.ds(z * NY, NY)] = block.astype(BF16).reshape(NY, 64, COLS)
        dz = order[k]
        w.send(("far_g", k), GG.at[blk(dz, 2)], FARG.at[k], up)
        w.send(("far_v", k), GV.at[blk(dz, 2)], FARV.at[k], down)
        w.send(("dir_g", k), GG.at[blk(dz, -1)], DIRG.at[k], down)
        w.send(("dir_v", k), GV.at[blk(dz, 1)], DIRV.at[k], up)

    def total(*parts):
        acc = parts[0].astype(F32)
        for part in parts[1:]:
            acc = acc + part.astype(F32)
        return acc

    def pass_on(k):
        dz = order[k]
        w.wait(("far_g", k), FARG.at[k], me)
        MIDG[k] = total(FARG[k], GG[blk(dz, 1)]).astype(BF16)
        w.send(("mid_g", k), MIDG.at[k], ENDG.at[k], up)
        w.wait(("far_v", k), FARV.at[k], me)
        MIDV[k] = total(FARV[k], GV[blk(dz, -1)]).astype(BF16)
        w.send(("mid_v", k), MIDV.at[k], ENDV.at[k], down)

    def row_done(k):
        own = blk(order[k], 0)
        w.wait(("dir_g", k), DIRG.at[k], me)
        w.wait(("mid_g", k), ENDG.at[k], me)
        RG[k] = total(GG[own], DIRG[k], ENDG[k]).astype(BF16)
        w.wait(("dir_v", k), DIRV.at[k], me)
        w.wait(("mid_v", k), ENDV.at[k], me)
        RV[k] = total(GV[own], DIRV[k], ENDV[k]).astype(BF16)

    chains = {
        "gr": (RG, ZRG, TRG, -1, 0, 8, right),
        "gl": (RG, ZLG, TLG, 1, 1, 7, left),
        "vr": (RV, ZRV, TRV, -1, 1, 7, right),
        "vl": (RV, ZLV, TLV, 1, 0, 8, left),
    }

    def hop(name, s):
        terms, landing, sums, way, start, length, to = chains[name]
        k = place[(way * (start + s)) % ZL]
        if s == 0:
            w.send((name, 0), terms.at[k], landing.at[0], to)
            return
        w.wait((name, s - 1), landing.at[s - 1], me)
        sums[s] = total(landing[s - 1], terms[k]).astype(BF16)
        w.send((name, s), sums.at[s], landing.at[s], to)

    hops = {
        0: [("gr", 0), ("vl", 0)],
        1: [("gl", 0), ("vl", 1)],
        2: [("gr", 1), ("vr", 0)],
        3: [("gl", 1), ("vl", 2)],
        4: [("gr", 2), ("vr", 1)],
        5: [("gl", 2), ("vl", 3)],
        6: [("gr", 3), ("vr", 2)],
        7: [("gr", 4), ("gl", 3), ("vl", 4), ("vr", 3)],
    }

    def input_terms(j):
        part = lax.dot_general(
            CG[...], WG[NY * j : NY * j + NY].reshape(FEAT, COLS),
            (((1,), (1,)), ((), ())), preferred_element_type=F32,
        ) + lax.dot_general(
            CV[...], WV[NY * j : NY * j + NY].reshape(FEAT, COLS),
            (((1,), (1,)), ((), ())), preferred_element_type=F32,
        )
        IP[j % 2, j // 2] = part.astype(BF16)

    def input_swap():
        for i in range(NX):
            w.send(("ip", i), IP.at[1 - c, i], IR.at[i], partner)

    def input_sums():
        for i in range(NX):
            w.wait(("ip", i), IR.at[i], me)
            IS[i] = total(IP[c, i], IR[i]).astype(BF16)
        for dx in (1, 3, 2):
            w.send(("is", dx), IS.at[lax.rem(x + dx, NX)], ISR.at[dx - 1], dev(x=x + dx))

    def input_done():
        for dx in (1, 3, 2):
            w.wait(("is", dx), ISR.at[dx - 1], me)
        din_ref[...] = total(IP[c, x], IR[x], ISR[0], ISR[1], ISR[2]).astype(BF16)

    def taps_y():
        for dy in (1, 2, 3):
            w.send(("ty", dy), TY.at[y], TY.at[y], dev(y=y + dy))

    def taps_z():
        for dy in (1, 2, 3):
            w.wait(("ty", dy), TY.at[lax.rem(y - dy + NY, NY)], me)
        TZ1[zo] = TY[0] + TY[1] + TY[2] + TY[3]
        for k in (1, 2, 3):
            w.send(("tz", k), TZ1.at[zo], TZ1.at[zo], z_near(k))

    def taps_pair(stage):
        if stage == 0:
            for k in (1, 2, 3):
                w.wait(("tz", k), TZ1.at[lax.rem(zo - k + 4, 4)], me)
            TB[0] = TZ1[0] + TZ1[1] + TZ1[2] + TZ1[3]
            w.send(("tb", 0), TB.at[0], TB.at[1], dev(z=zg + side))
        else:
            w.wait(("tb", 0), TB.at[1], me)
            TB[2] = TB[0] + TB[1]
            w.send(("tb", 1), TB.at[2], TB.at[3], dev(z=zg - side))

    def taps_spread():
        w.wait(("tb", 1), TB.at[3], me)
        TT[tp] = (TB[2] + TB[3]) * factor
        for k in range(1, 8):
            w.send(("tt", k), TT.at[tp], TT.at[tp], tp_peer(k))

    def taps_done():
        for k in range(1, 8):
            w.wait(("tt", k), TT.at[lax.rem(tp - k + 8, 8)], me)
        tout_ref[...] = TT[...]

    make_blocks(0)
    make_blocks(1)
    make_blocks(2)
    taps_y()
    pass_on(0)
    make_blocks(3)
    pass_on(1)
    row_done(0)
    for h in hops[0]:
        hop(*h)
    make_blocks(4)
    for j in range(4):
        input_terms(j)
    pass_on(2)
    row_done(1)
    for h in hops[1]:
        hop(*h)
    make_blocks(5)
    for j in range(4, 8):
        input_terms(j)
    input_swap()
    taps_z()
    pass_on(3)
    row_done(2)
    for h in hops[2]:
        hop(*h)
    make_blocks(6)
    make_blocks(7)
    input_sums()
    pass_on(4)
    row_done(3)
    for h in hops[3]:
        hop(*h)
    taps_pair(0)
    pass_on(5)
    row_done(4)
    for h in hops[4]:
        hop(*h)
    pass_on(6)
    row_done(5)
    for h in hops[5]:
        hop(*h)
    taps_pair(1)
    pass_on(7)
    row_done(6)
    for h in hops[6]:
        hop(*h)
    taps_spread()
    row_done(7)
    for h in hops[7]:
        hop(*h)
    input_done()
    for s in (5, 6, 7):
        for name in ("gr", "gl", "vl", "vr"):
            hop(name, s if chains[name][5] == 8 else s - 1)
    taps_done()
    own_k = place[0]
    w.wait(("gr", 7), ZRG.at[7], me)
    w.wait(("gl", 6), ZLG.at[6], me)
    dg_ref[...] = total(RG[own_k], ZRG[7], ZLG[6]) * factor
    w.wait(("vl", 7), ZLV.at[7], me)
    w.wait(("vr", 6), ZRV.at[6], me)
    dv_ref[...] = total(RV[own_k], ZLV[7], ZRV[6]) * factor
    w.drain()


COPIES = 320


def shards(inputs, gate_proj, value_proj, gate_taps, value_taps, out_grad):
    rows, cols = gate_proj.shape
    start = lax.axis_index("tp") * cols
    taps = jnp.stack(
        [
            lax.dynamic_slice_in_dim(gate_taps, start, cols, 1),
            lax.dynamic_slice_in_dim(value_taps, start, cols, 1),
        ]
    )
    factor = float(TOK * NY * NZ) ** (-0.5)
    unit = (rows, cols)
    vm = pltpu.VMEM
    scratch = [
        vm((8, EXT, FEAT), BF16),
        vm((32, *unit), BF16),
        vm((32, *unit), BF16),
        vm((384, TOK), BF16),
        vm((EXT, cols), BF16),
        vm((EXT + 16, cols), F32),
        vm((EXT + 16, cols), F32),
        vm((EXT + 16, cols), F32),
        vm((EXT + 16, cols), F32),
        vm((TOK, cols), BF16),
        vm((TOK, cols), BF16),
        vm((32, *unit), BF16),
        vm((32, *unit), BF16),
    ]
    scratch += [vm((8, *unit), BF16) for _ in range(10)]
    scratch += [vm((8, *unit), BF16) for _ in range(8)]
    scratch += [
        vm((2, NX, TOK, FEAT), BF16),
        vm((NX, TOK, FEAT), BF16),
        vm((NX, TOK, FEAT), BF16),
        vm((3, TOK, FEAT), BF16),
        vm((4, 8, cols), F32),
        vm((4, 8, cols), F32),
        vm((4, 8, cols), F32),
        vm((8, 8, cols), F32),
        pltpu.SemaphoreType.DMA((COPIES,)),
        pltpu.SemaphoreType.DMA((COPIES,)),
        pltpu.SemaphoreType.DMA((4,)),
    ]
    hbm = pl.BlockSpec(memory_space=pl.ANY)
    vmem = pl.BlockSpec(memory_space=pltpu.VMEM)
    din, dg, dv, tout = pl.pallas_call(
        functools.partial(kernel, factor),
        out_shape=(
            jax.ShapeDtypeStruct((TOK, FEAT), BF16),
            jax.ShapeDtypeStruct(unit, F32),
            jax.ShapeDtypeStruct(unit, F32),
            jax.ShapeDtypeStruct((8, 8, cols), F32),
        ),
        in_specs=[hbm, hbm, hbm, hbm, vmem],
        out_specs=(vmem, vmem, vmem, vmem),
        scratch_shapes=scratch,
        compiler_params=pltpu.CompilerParams(
            collective_id=0, has_side_effects=True, vmem_limit_bytes=56 * 1024 * 1024
        ),
    )(inputs[0], gate_proj, value_proj, jnp.swapaxes(out_grad[0], 0, 1), taps)
    taps_all = jnp.moveaxis(tout[:, :6], 0, 1).reshape(6, 8 * cols)
    return din[None], dg, dv, taps_all[:3], taps_all[3:]


def solution(mesh):
    return jax.shard_map(
        shards,
        mesh=mesh,
        in_specs=(P("rep", "fs", "tp"), P("fs", "tp"), P("fs", "tp"), P(), P(), P("rep", "fs", "tp")),
        out_specs=(P("rep", "fs", "tp"), P("fs", "tp"), P("fs", "tp"), P(), P()),
        check_vma=False,
    )
```

time: 407 us -> 107 us (0.26)
  the two profiles are of different devices: /device:TPU:32 before, /device:TPU:24 now
where the time goes in v1:
time: 107 us; the launch traced here: 106 us
  Pallas kernels  99.5 us (93%)
  local copies, waits for them, and re-layouts  5.69 us (5%)
    pallas_call x1, Pallas kernels, shards(): pl.pallas_call(functools.partial(kernel, factor), out_shape=(jax.ShapeDty...  99.5 us
    unnamed x9, local copies, waits for them, and re-layouts  2.53 us

profile of v1, /device:TPU:24, one launch (start us, length us, event | category | flops | bytes accessed | tf_op | source)
XLA Modules:
  0.0 106.5 jit_solution(985253233082317095)
XLA Ops:
  0.6 0.8 dynamic-slice_bitcast_fusion
  1.4 0.6 pad_maximum_fusion.taps_ref
  2.0 99.5 %shard_map.101 = (bf16[384,256]{1,0:T(8,128)(2,1)}, f32[64,352]{1,0:T(8,128)}, f32[64,352]{1,0:T(8,128)}, f32[8,8,352]{2,1,0:T(8,128)}) custom-call(bf16[384,256]{1,0:T(8,128)(2,1)} %bitcast.13, bf16[64,352]{1,0:T(8,128)(2,1)} %wg_hbm.1, bf16[64,352]{1,0:T(8,128)(2,1)} %wv_hbm.1, bf16[352,384]{1,0:T(8,128)(2,1)} %bitcast.11, ...), custom_call_target="tpu_custom_call" | custom-call | tf_op jit(solution)/shard_map/pallas_call | solution.py:578
  101.6 0.9 slice_bitcast_fusion
  102.5 0.0 copy-start
  102.5 0.7 slice.17
  103.2 0.7 slice.19
  103.9 0.0 copy-done
  103.9 0.0 copy-start.2
  103.9 0.7 copy.16
  104.6 0.3 copy-done.2
  104.9 0.0 copy-start.1
  104.9 0.6 copy.17
  105.5 0.3 copy-done.1
  105.8 0.6 copy.18
  (3 shorter events, 0.0 us)
Async XLA Ops:
  102.5 1.5 %copy-start = (bf16[384,256]{1,0:T(8,128)(2,1)S(1)}, bf16[384,256]{1,0:T(8,128)(2,1)}, u32[]{:S(2)}) copy-start(bf16[384,256]{1,0:T(8,128)(2,1)} %get-tuple-element.9) | copy-start | bytes 589828
  103.9 1.0 copy-start.2
  104.9 0.9 copy-start.1

commit v2 on v1

v2 whole, which is shorter than its diff:
```python
import functools

import jax
import jax.numpy as jnp
from jax import lax
from jax.experimental import pallas as pl
from jax.experimental.pallas import tpu as pltpu
from jax.sharding import PartitionSpec as P

MESH = pl.DeviceIdType.MESH
BF16 = jnp.bfloat16
F32 = jnp.float32

NX, NC, NY, NZ = 4, 2, 4, 16
ZL = 8
TOK = 384
COLS = 352
FEAT = 256
EDGE = 16
EXT = TOK + 2 * EDGE


def right_reach(r):
    return 4 if r < 2 else 3


class Wires:
    def __init__(self, send_sems, recv_sems):
        self.send_sems, self.recv_sems = send_sems, recv_sems
        self.index = {}
        self.count = dict.fromkeys(("unit", "tile", "edge", "og", "taps"), 0)

    def at(self, key):
        return self.index.setdefault(key, len(self.index))

    def copy(self, key, src, dst, to, kind):
        return pltpu.make_async_remote_copy(
            src_ref=src,
            dst_ref=dst,
            send_sem=self.send_sems.at[list(self.count).index(kind)],
            recv_sem=self.recv_sems.at[self.at(key)],
            device_id=to,
            device_id_type=MESH,
        )

    def send(self, key, src, dst, to, kind="unit"):
        self.count[kind] += 1
        self.copy(key, src, dst, to, kind).start()

    def wait(self, key, dst, to, kind="unit"):
        self.copy(key, dst, dst, to, kind).wait_recv()

    def drain(self, spans, to):
        for kind, span in spans.items():
            whole = span(self.count[kind])
            self.copy(("drain",), whole, whole, to, kind).wait_send()


def kernel(
    factor,
    x_hbm, wg_hbm, wv_hbm, gt_hbm, vt_hbm, ogt_hbm,
    din_hbm, dg_hbm, dv_hbm, tout_hbm,
    X, U, XB, TS, GT, VT, OGT, OG, PG, PV, KG, KV, CG, CV, DIN, DG, DV,
    send_sems, recv_sems, local_sems,
):
    def parts_of(pool, sizes):
        first, parts = 0, []
        for size in sizes:
            parts.append(pool.at[pl.ds(first, size)])
            first += size
        return parts

    WG, WV, GG, GV, *rest = parts_of(U, [32] * 4 + [8] * 18)
    FAR, DIR, MID, END, RED = ({"g": rest[2 * i], "v": rest[2 * i + 1]} for i in range(5))
    ZRG, ZLG, ZRV, ZLV = rest[10:14]
    SUMS = dict(zip(("gr", "gl", "vr", "vl"), rest[14:18]))
    IP, IR, IS, ISR = parts_of(XB, [2 * NX, NX, NX, 3])
    TY, TZ1, TB, TT = parts_of(TS, [4, 4, 4, 8])
    rep, fs, tp = lax.axis_index("rep"), lax.axis_index("fs"), lax.axis_index("tp")
    zl, y = lax.div(fs, NY), lax.rem(fs, NY)
    x, c = lax.div(tp, NC), lax.rem(tp, NC)
    zg = rep * ZL + zl

    def dev(x=x, c=c, y=y, z=zg):
        z = lax.rem(z + NZ, NZ)
        return (
            lax.div(z, ZL),
            lax.rem(z, ZL) * NY + lax.rem(y + NY, NY),
            lax.rem(x + NX, NX) * NC + c,
        )

    def blk(dz, dy):
        return lax.rem(zl + dz + ZL, ZL) * NY + lax.rem(y + dy + NY, NY)

    def zrow(dz):
        return lax.rem(zl + dz + 2 * ZL, ZL)

    me = dev()
    right, left = dev(z=zg + 1), dev(z=zg - 1)
    up, down = dev(y=y + 1), dev(y=y - 1)
    partner = dev(c=1 - c)
    after_z = zg + lax.div(y + 1, NY)
    after = dev(y=y + 1, z=after_z)
    before_z = zg - 1 + lax.div(y + NY - 1, NY)
    before = dev(y=y - 1, z=before_z)

    def tp_peer(k):
        return (rep, fs, lax.rem(tp + k + 8, 8))

    zq, zo = lax.div(zg, 4), lax.rem(zg, 4)
    side = 4 * (1 - 2 * lax.rem(zq, 2))

    def z_near(k):
        return dev(z=zq * 4 + lax.rem(zo + k, 4))

    own = blk(0, 0)
    loads = [
        pltpu.make_async_copy(wg_hbm, WG.at[own], local_sems.at[0]),
        pltpu.make_async_copy(wv_hbm, WV.at[own], local_sems.at[1]),
        pltpu.make_async_copy(x_hbm, X.at[tp, pl.ds(EDGE, TOK)], local_sems.at[2]),
        pltpu.make_async_copy(ogt_hbm, OGT.at[pl.ds(0, COLS)], local_sems.at[3]),
        pltpu.make_async_copy(gt_hbm, GT, local_sems.at[4]),
        pltpu.make_async_copy(vt_hbm, VT, local_sems.at[5]),
    ]
    for load in loads:
        load.start()

    barrier = pltpu.get_barrier_semaphore()
    peers = [tp_peer(k) for k in range(1, 8)]
    peers += [dev(y=y + k) for k in (1, 2, 3)]
    peers += [right, left, after, before]
    peers += [z_near(k) for k in (1, 2, 3)]
    peers += [dev(z=zg + 4), dev(z=zg - 4)]
    for peer in peers:
        pl.semaphore_signal(barrier, inc=1, device_id=peer, device_id_type=MESH)
    pl.semaphore_wait(barrier, len(peers))

    w = Wires(send_sems, recv_sems)

    loads[0].wait()
    for dy in (1, 3, 2):
        w.send(("gy", dy), WG.at[own], WG.at[own], dev(y=y + dy))
    loads[1].wait()
    w.send(("vz", 1, 1), WV.at[own], WV.at[own], right)
    w.send(("vz", -1, 1), WV.at[own], WV.at[own], left)
    w.send(("gz", 0, 1, 1), WG.at[own], WG.at[own], right)
    w.send(("gz", 0, -1, 1), WG.at[own], WG.at[own], left)
    loads[2].wait()
    head, tail = X.at[tp, pl.ds(EDGE, EDGE)], X.at[tp, pl.ds(TOK, EDGE)]
    lo, hi = pl.ds(0, EDGE), pl.ds(TOK + EDGE, EDGE)
    w.send(("hx", 1), tail, X.at[tp, lo], after, "edge")
    w.send(("hx", -1), head, X.at[tp, hi], before, "edge")
    mine = X.at[tp, pl.ds(EDGE, TOK)]
    for dx in (1, 3, 2):
        w.send(("x", dx), mine, mine, dev(x=x + dx), "tile")
    w.send(("xp", 0), mine, mine, partner, "tile")
    w.send(("vy", 0, 1), WV.at[own], WV.at[own], up)
    w.send(("vy", 0, -1), WV.at[own], WV.at[own], down)

    def out_grad_rows():
        loads[3].wait()
        for i in range(3):
            for j in range(3):
                block = OGT[128 * i : 128 * i + 128, 128 * j : 128 * j + 128].astype(F32)
                cols = min(128, COLS - 128 * i)
                OG[EDGE + 128 * j : EDGE + 128 * j + 128, 128 * i : 128 * i + cols] = (
                    block.T[:, :cols].astype(BF16)
                )

    def gate_chunk(z, first=False):
        part = jnp.dot(
            X[z],
            WG[pl.ds(z * NY, NY)].reshape(FEAT, COLS),
            preferred_element_type=F32,
        )
        if first:
            PG[8 : 8 + EXT] = part
        else:
            PG[8 : 8 + EXT] += part

    def value_chunk(z, first=False):
        part = jnp.dot(
            X[z],
            WV[pl.ds(z * NY, NY)].reshape(FEAT, COLS),
            preferred_element_type=F32,
        )
        if first:
            PV[8 : 8 + EXT] = part
        else:
            PV[8 : 8 + EXT] += part

    def x_arrived(dx):
        slot = X.at[lax.rem(x - dx + NX, NX) * NC + c, pl.ds(EDGE, TOK)]
        w.wait(("x", dx), slot, me, "tile")
        w.send(("xp", dx), slot, slot, partner, "tile")

    def xp_arrived(dx):
        slot = X.at[lax.rem(x - dx + NX, NX) * NC + 1 - c, pl.ds(EDGE, TOK)]
        w.wait(("xp", dx), slot, me, "tile")

    def edges_spread():
        w.wait(("hx", 1), X.at[tp, lo], me, "edge")
        w.wait(("hx", -1), X.at[tp, hi], me, "edge")
        for k in range(1, 8):
            w.send(("hl",), X.at[tp, lo], X.at[tp, lo], tp_peer(k), "edge")
            w.send(("hl",), X.at[tp, hi], X.at[tp, hi], tp_peer(k), "edge")

    def edges_done():
        w.wait(("hl",), X.at[0, pl.ds(0, 14 * EDGE)], me, "edge")

    def gate_y(dy):
        unit = WG.at[blk(0, -dy)]
        w.wait(("gy", dy), unit, me)
        w.send(("gz", 4 - dy, 1, 1), unit, unit, right)
        w.send(("gz", 4 - dy, -1, 1), unit, unit, left)

    def gate_z(r, d):
        for way, reach, to in ((1, right_reach(r), right), (-1, 7 - right_reach(r), left)):
            if d <= reach:
                unit = WG.at[blk(-way * d, r)]
                w.wait(("gz", r, way, d), unit, me)
                if d < reach:
                    w.send(("gz", r, way, d + 1), unit, unit, to)

    def value_z(d):
        for way, reach, to in ((1, 4, right), (-1, 3, left)):
            if d <= reach:
                dz = -way * d
                unit = WV.at[blk(dz, 0)]
                w.wait(("vz", way, d), unit, me)
                if d < reach:
                    w.send(("vz", way, d + 1), unit, unit, to)
                w.send(("vy", dz, 1), unit, unit, up)
                w.send(("vy", dz, -1), unit, unit, down)

    def value_y(dz):
        from_down, from_up = WV.at[blk(dz, -1)], WV.at[blk(dz, 1)]
        w.wait(("vy", dz, 1), from_down, me)
        if dz % 2 == 0:
            w.send(("vf", dz), from_down, from_down, up)
        w.wait(("vy", dz, -1), from_up, me)
        if dz % 2 == 1:
            w.send(("vf", dz), from_up, from_up, down)

    def value_row(dz, first=False):
        w.wait(("vf", dz), WV.at[blk(dz, 2)], me)
        value_chunk(zrow(dz), first)

    value_z(1)
    gate_y(1)
    gate_y(3)
    edges_spread()
    gate_y(2)
    gate_z(0, 1)
    value_y(0)
    value_z(2)
    gate_z(3, 1)
    gate_z(1, 1)
    gate_z(2, 1)
    value_y(1)
    value_y(-1)
    out_grad_rows()
    gate_z(0, 2)
    value_z(3)
    w.send(("og", 1), OG.at[pl.ds(TOK, EDGE)], OG.at[lo], after, "og")
    w.send(("og", -1), OG.at[pl.ds(EDGE, EDGE)], OG.at[hi], before, "og")
    x_arrived(1)
    x_arrived(3)
    gate_z(3, 2)
    value_y(2)
    value_y(-2)
    gate_z(1, 2)
    gate_z(2, 2)
    gate_z(0, 3)
    value_z(4)
    x_arrived(2)
    gate_z(3, 3)
    value_y(3)
    value_y(-3)
    gate_z(1, 3)
    for dx in (0, 1, 3, 2):
        xp_arrived(dx)
    edges_done()
    gate_chunk(zrow(0), first=True)
    gate_chunk(zrow(1))
    gate_z(2, 3)
    gate_chunk(zrow(-1))
    value_row(0, first=True)
    gate_z(0, 4)
    gate_chunk(zrow(2))
    gate_chunk(zrow(-2))
    value_y(-4)
    gate_z(3, 4)
    value_row(1)
    value_row(-1)
    gate_z(1, 4)
    value_row(2)
    value_row(-2)
    gate_z(2, 4)
    gate_chunk(zrow(3))
    gate_chunk(zrow(-3))
    gate_chunk(zrow(4))
    value_row(3)
    value_row(-3)
    value_row(-4)
    w.wait(("og", 1), OG.at[lo], me, "og")
    w.wait(("og", -1), OG.at[hi], me, "og")

    not_first, not_last = fs > 0, fs < NY * ZL - 1
    for ref in (PG, PV):
        ref[8 : 8 + EDGE] = jnp.where(not_first, ref[8 : 8 + EDGE], 0.0)
        ref[8 + EDGE + TOK : 8 + EXT] = jnp.where(not_last, ref[8 + EDGE + TOK : 8 + EXT], 0.0)
    OG[:EDGE] = jnp.where(not_first, OG[:EDGE].astype(F32), 0.0).astype(BF16)
    OG[EDGE + TOK :] = jnp.where(not_last, OG[EDGE + TOK :].astype(F32), 0.0).astype(BF16)

    loads[4].wait()
    loads[5].wait()
    taps = jnp.concatenate([GT[...], VT[...], jnp.zeros((2, 8 * COLS), F32)], axis=0)
    taps = pltpu.roll(taps, lax.rem((8 - tp) * COLS, 8 * COLS), axis=1)[:, :COLS]
    g0, g1, g2, v0, v1, v2 = (taps[k : k + 1] for k in range(6))

    def rounded(value):
        return value.astype(BF16).astype(F32)

    def cot_rows(i):
        base = pl.multiple_of(i * 16, 16)
        gate = rounded(PG[pl.ds(base, 32)])
        value = rounded(PV[pl.ds(base, 32)])
        gm, gz, gp = gate[7:23], gate[8:24], gate[9:25]
        vm, vz, vp = value[7:23], value[8:24], value[9:25]
        gate_mix = g0 * gm + g1 * gz + g2 * gp
        value_mix = v0 * vm + v1 * vz + v2 * vp
        grad = OG[pl.ds(base, 16)].astype(F32)
        s = jax.nn.sigmoid(gate_mix)
        gate_cot = grad * value_mix * (s * (1.0 + gate_mix * (1.0 - s)))
        value_cot = grad * (gate_mix * s)
        KG[pl.ds(base + 8, 16)] = gate_cot
        KV[pl.ds(base + 8, 16)] = value_cot
        return [
            (p * k).reshape(2, 8, COLS).sum(axis=0)
            for p, k in (
                (gm, gate_cot), (gz, gate_cot), (gp, gate_cot),
                (vm, value_cot), (vz, value_cot), (vp, value_cot),
            )
        ]

    cot_rows(0)
    cot_rows(TOK // 16 + 1)
    zero = jnp.zeros((8, COLS), F32)
    tap_sums = lax.fori_loop(
        1, TOK // 16 + 1,
        lambda i, sums: tuple(a + b for a, b in zip(sums, cot_rows(i))),
        (zero,) * 6,
    )

    def back_rows(i, carry):
        base = pl.multiple_of(i * 16, 16)
        out = pl.ds(pl.multiple_of(i * 16 - 16, 16), 16)
        for source, target, (t0, t1, t2) in ((KG, CG, (g0, g1, g2)), (KV, CV, (v0, v1, v2))):
            cot = source[pl.ds(base, 32)]
            target[out] = (t0 * cot[9:25] + t1 * cot[8:24] + t2 * cot[7:23]).astype(BF16)
        return carry

    lax.fori_loop(1, TOK // 16 + 1, back_rows, 0)

    rows = [jnp.sum(part, axis=0, keepdims=True) for part in tap_sums]
    TY[y] = jnp.concatenate(rows + [jnp.zeros((2, COLS), F32)], axis=0)

    order = (0, 1, -1, 2, -2, 3, -3, 4)
    place = {dz % ZL: k for k, dz in enumerate(order)}
    COT, TERMS = {"g": CG, "v": CV}, {"g": GG, "v": GV}

    def turn(k):
        return (1, up, down) if k % 2 == 0 else (-1, down, up)

    def make_blocks(h, k):
        dz = order[k]
        z = zrow(dz)
        block = lax.dot_general(
            X[z, EDGE : EDGE + TOK, :], COT[h][...],
            (((0,), (0,)), ((), ())), preferred_element_type=F32,
        )
        TERMS[h][pl.ds(z * NY, NY)] = block.astype(BF16).reshape(NY, 64, COLS)
        way, onward, back = turn(k)
        w.send(("far", h, k), TERMS[h].at[blk(dz, 2)], FAR[h].at[k], onward)
        w.send(("dir", h, k), TERMS[h].at[blk(dz, -way)], DIR[h].at[k], back)

    def total(*parts):
        acc = parts[0].astype(F32)
        for part in parts[1:]:
            acc = acc + part.astype(F32)
        return acc

    def pass_on(h, k):
        way, onward, back = turn(k)
        w.wait(("far", h, k), FAR[h].at[k], me)
        MID[h][k] = total(FAR[h][k], TERMS[h][blk(order[k], way)]).astype(BF16)
        w.send(("mid", h, k), MID[h].at[k], END[h].at[k], onward)

    def row_done(h, k):
        w.wait(("dir", h, k), DIR[h].at[k], me)
        w.wait(("mid", h, k), END[h].at[k], me)
        RED[h][k] = total(TERMS[h][blk(order[k], 0)], DIR[h][k], END[h][k]).astype(BF16)

    chains = {
        "gr": ("g", ZRG, -1, 0, 8, right, None),
        "gl": ("g", ZLG, 1, 1, 7, left, None),
        "vr": ("v", ZRV, -1, 1, 7, right, dev(z=zg + 4)),
        "vl": ("v", ZLV, 1, 0, 8, left, dev(z=zg - 4)),
    }

    def hop(name, s):
        h, landing, way, start, length, to, end = chains[name]
        k = place[(way * (start + s)) % ZL]
        cut = length - 4 if end is not None else None
        first = s == 0 or (cut is not None and s == cut + 1)
        slot = landing.at[s]
        if first:
            w.send((name, s), RED[h].at[k], slot, to)
            return
        w.wait((name, s - 1), landing.at[s - 1], me)
        SUMS[name][s] = total(landing[s - 1], RED[h][k]).astype(BF16)
        w.send((name, s), SUMS[name].at[s], slot, end if s == cut else to)

    def finish(h, names, out):
        parts = [RED[h][place[0]]]
        for name in names:
            _, landing, _, _, length, _, end = chains[name]
            for s in (length - 1,) if end is None else (length - 1, length - 4):
                w.wait((name, s), landing.at[s], me)
                parts.append(landing[s])
        out[...] = total(*parts) * factor

    def input_terms(j):
        part = lax.dot_general(
            CG[...], WG[NY * j : NY * j + NY].reshape(FEAT, COLS),
            (((1,), (1,)), ((), ())), preferred_element_type=F32,
        ) + lax.dot_general(
            CV[...], WV[NY * j : NY * j + NY].reshape(FEAT, COLS),
            (((1,), (1,)), ((), ())), preferred_element_type=F32,
        )
        IP[NX * (j % 2) + j // 2] = part.astype(BF16)

    def input_swap():
        for i in range(NX):
            w.send(("ip", i), IP.at[NX * (1 - c) + i], IR.at[i], partner, "tile")

    def input_sums():
        for i in range(NX):
            w.wait(("ip", i), IR.at[i], me, "tile")
            IS[i] = total(IP[NX * c + i], IR[i]).astype(BF16)
        for dx in (1, 3, 2):
            w.send(("is", dx), IS.at[lax.rem(x + dx, NX)], ISR.at[dx - 1], dev(x=x + dx), "tile")

    results = []

    def put_out(source, target):
        copy = pltpu.make_async_copy(source, target, local_sems.at[6 + len(results)])
        copy.start()
        results.append(copy)

    def input_done():
        for dx in (1, 3, 2):
            w.wait(("is", dx), ISR.at[dx - 1], me, "tile")
        DIN[...] = total(IP[NX * c + x], IR[x], ISR[0], ISR[1], ISR[2]).astype(BF16)
        put_out(DIN, din_hbm)

    def taps_y():
        for dy in (1, 2, 3):
            w.send(("ty",), TY.at[y], TY.at[y], dev(y=y + dy), "taps")

    def taps_z():
        w.wait(("ty",), TY.at[pl.ds(0, 3)], me, "taps")
        TZ1[zo] = TY[0] + TY[1] + TY[2] + TY[3]
        for k in (1, 2, 3):
            w.send(("tz",), TZ1.at[zo], TZ1.at[zo], z_near(k), "taps")

    def taps_pair(stage):
        if stage == 0:
            w.wait(("tz",), TZ1.at[pl.ds(0, 3)], me, "taps")
            TB[0] = TZ1[0] + TZ1[1] + TZ1[2] + TZ1[3]
            w.send(("tb", 0), TB.at[0], TB.at[1], dev(z=zg + side), "taps")
        else:
            w.wait(("tb", 0), TB.at[1], me, "taps")
            TB[2] = TB[0] + TB[1]
            w.send(("tb", 1), TB.at[2], TB.at[3], dev(z=zg - side), "taps")

    def taps_spread():
        w.wait(("tb", 1), TB.at[3], me, "taps")
        TT[tp] = (TB[2] + TB[3]) * factor
        for k in range(1, 8):
            w.send(("tt",), TT.at[tp], TT.at[tp], tp_peer(k), "taps")

    def taps_done():
        w.wait(("tt",), TT.at[pl.ds(0, 7)], me, "taps")
        put_out(TT, tout_hbm)

    steps = [(h, k) for h in "gv" for k in range(ZL)]
    after_row = {
        ("g", 0): [("gr", 0)],
        ("g", 1): [("gl", 0)],
        ("g", 2): [("gr", 1)],
        ("g", 3): [("gl", 1)],
        ("g", 4): [("gr", 2)],
        ("g", 5): [("gl", 2)],
        ("g", 6): [("gr", 3)],
        ("g", 7): [("gl", 3), ("gr", 4)],
        ("v", 0): [("vl", 0)],
        ("v", 1): [("vl", 1), ("gl", 4), ("gr", 5)],
        ("v", 2): [("vr", 0)],
        ("v", 3): [("vl", 2), ("gl", 5), ("gr", 6)],
        ("v", 4): [("vr", 1)],
        ("v", 5): [("vl", 3), ("vr", 4)],
        ("v", 6): [("vr", 2), ("vl", 5), ("gl", 6), ("gr", 7)],
        ("v", 7): [("vl", 4), ("vr", 3)],
    }
    extra = {2: [taps_y], 6: [taps_z], 10: [lambda: taps_pair(0)], 11: [input_swap], 13: [lambda: taps_pair(1)],
             14: [input_sums], 16: [taps_spread]}
    for j in range(8):
        extra.setdefault(3 + j, []).append(functools.partial(input_terms, j))
    for i in range(len(steps) + 5):
        if i < len(steps):
            make_blocks(*steps[i])
        if 0 <= i - 3 < len(steps):
            pass_on(*steps[i - 3])
        if 0 <= i - 5 < len(steps):
            row_done(*steps[i - 5])
            for name, s in after_row[steps[i - 5]]:
                hop(name, s)
        for run in extra.get(i, ()):
            run()
    hop("vl", 6)
    hop("vr", 5)
    input_done()
    taps_done()
    finish("g", ("gr", "gl"), DG)
    put_out(DG, dg_hbm)
    hop("vl", 7)
    hop("vr", 6)
    finish("v", ("vl", "vr"), DV)
    put_out(DV, dv_hbm)
    w.drain(
        {
            "unit": lambda n: U.at[pl.ds(0, n)],
            "tile": lambda n: XB.at[pl.ds(0, n)],
            "edge": lambda n: X.at[0, pl.ds(0, n * EDGE)],
            "og": lambda n: OG.at[pl.ds(0, n * EDGE)],
            "taps": lambda n: TS.at[pl.ds(0, n)],
        },
        me,
    )
    for copy in results:
        copy.wait()
    if len(w.index) != RECEIVES:
        raise ValueError(str(len(w.index)))


RECEIVES = 165


def finisher(din_ref, dg_ref, dv_ref, tt_ref, din_out, dg_out, dv_out, tg_out, tv_out):
    din_out[...] = din_ref[...]
    dg_out[...] = dg_ref[...]
    dv_out[...] = dv_ref[...]
    taps = jnp.concatenate([tt_ref[i] for i in range(8)], axis=1)
    tg_out[...] = taps[0:3]
    tv_out[...] = taps[3:6]


def shards(inputs, gate_proj, value_proj, gate_taps, value_taps, out_grad):
    unit = gate_proj.shape
    cols = unit[1]
    factor = float(TOK * NY * NZ) ** (-0.5)
    vm = pltpu.VMEM
    scratch = [
        vm((8, EXT, FEAT), BF16),
        vm((272, *unit), BF16),
        vm((4 * NX + 3, TOK, FEAT), BF16),
        vm((20, 8, cols), F32),
        vm(gate_taps.shape, F32),
        vm(gate_taps.shape, F32),
        vm((384, TOK), BF16),
        vm((EXT, cols), BF16),
        vm((EXT + 16, cols), F32),
        vm((EXT + 16, cols), F32),
        vm((EXT + 16, cols), F32),
        vm((EXT + 16, cols), F32),
        vm((TOK, cols), BF16),
        vm((TOK, cols), BF16),
        vm((TOK, FEAT), BF16),
        vm(unit, F32),
        vm(unit, F32),
        pltpu.SemaphoreType.DMA((5,)),
        pltpu.SemaphoreType.DMA((RECEIVES,)),
        pltpu.SemaphoreType.DMA((10,)),
    ]
    anywhere = pl.BlockSpec(memory_space=pl.ANY)
    vmem = pl.BlockSpec(memory_space=pltpu.VMEM)
    tile = jax.ShapeDtypeStruct((TOK, FEAT), BF16)
    grad = jax.ShapeDtypeStruct(unit, F32)
    tap = jax.ShapeDtypeStruct(gate_taps.shape, F32)
    sums = pl.pallas_call(
        functools.partial(kernel, factor),
        out_shape=(tile, grad, grad, jax.ShapeDtypeStruct((8, 8, cols), F32)),
        in_specs=[anywhere] * 6,
        out_specs=(anywhere,) * 4,
        scratch_shapes=scratch,
        compiler_params=pltpu.CompilerParams(
            collective_id=0, has_side_effects=True, vmem_limit_bytes=65000 * 1024
        ),
    )(inputs[0], gate_proj, value_proj, gate_taps, value_taps, jnp.swapaxes(out_grad[0], 0, 1))
    din, dg, dv, tg, tv = pl.pallas_call(
        finisher,
        out_shape=(tile, grad, grad, tap, tap),
        in_specs=[vmem] * 4,
        out_specs=(vmem,) * 5,
    )(*sums)
    return din[None], dg, dv, tg, tv


def solution(mesh):
    return jax.shard_map(
        shards,
        mesh=mesh,
        in_specs=(P("rep", "fs", "tp"), P("fs", "tp"), P("fs", "tp"), P(), P(), P("rep", "fs", "tp")),
        out_specs=(P("rep", "fs", "tp"), P("fs", "tp"), P("fs", "tp"), P(), P()),
        check_vma=False,
    )
```

time: 107 us -> 95.7 us (0.89)
  local copies, waits for them, and re-layouts: 5.69 us -> 0 us
  Pallas kernels: 99.5 us -> 94.3 us
    pallas_call x1 -> x2, Pallas kernels: 99.5 us -> 94.3 us  [the longest x1 92.5 us: shards(): pl.pallas_call(functools.partial(kernel, factor), out_shape=(tile, grad,...]
    unnamed x9 -> x0, local copies, waits for them, and re-layouts: 2.53 us -> none
    slice x5 -> x0, local copies, waits for them, and re-layouts: 1.46 us -> none  [shards(): return (din[None], dg, dv, taps_all[:3], taps_all[3:])]
where the time goes in v2:
time: 95.7 us; the launch traced here: 95 us
  Pallas kernels  94.3 us (99%)
    pallas_call x1, Pallas kernels, shards(): pl.pallas_call(functools.partial(kernel, factor), out_shape=(tile, grad,...  92.5 us

profile of v2, /device:TPU:24, one launch (start us, length us, event | category | flops | bytes accessed | tf_op | source)
XLA Modules:
  0.0 95.0 jit_solution(7650315299016342665)
XLA Ops:
  0.6 92.5 %shard_map.101 = (bf16[384,256]{1,0:T(8,128)(2,1)}, f32[64,352]{1,0:T(8,128)}, f32[64,352]{1,0:T(8,128)}, f32[8,8,352]{2,1,0:T(8,128)}) custom-call(bf16[384,256]{1,0:T(8,128)(2,1)} %bitcast.6, bf16[64,352]{1,0:T(8,128)(2,1)} %wg_hbm.1, bf16[64,352]{1,0:T(8,128)(2,1)} %wv_hbm.1, f32[3,2816]{1,0:T(4,128)} %gt_hbm.1, f32[3,2816]{1,0:T(4,128)} %vt_hbm.1, ...), custom_call_target="tpu_custom_call" | custom-call | tf_op jit(solution)/shard_map/pallas_call | solution.py:602
  93.1 1.9 %shard_map.102 = (bf16[384,256]{1,0:T(8,128)(2,1)}, f32[64,352]{1,0:T(8,128)}, f32[64,352]{1,0:T(8,128)}, f32[3,2816]{1,0:T(4,128)}, f32[3,2816]{1,0:T(4,128)}) custom-call(bf16[384,256]{1,0:T(8,128)(2,1)} %get-tuple-element.14.din_ref, f32[64,352]{1,0:T(8,128)} %get-tuple-element.15.dg_ref, f32[64,352]{1,0:T(8,128)} %get-tuple-element.16.dv_ref, ...), custom_call_target="tpu_custom_call" | custom-call | tf_op jit(solution)/shard_map/pallas_call | solution.py:612

commit v3 on v2

--- a/solution.py
+++ b/solution.py
@@ -72,8 +72,8 @@
 
     WG, WV, GG, GV, *rest = parts_of(U, [32] * 4 + [8] * 18)
     FAR, DIR, MID, END, RED = ({"g": rest[2 * i], "v": rest[2 * i + 1]} for i in range(5))
-    ZRG, ZLG, ZRV, ZLV = rest[10:14]
-    SUMS = dict(zip(("gr", "gl", "vr", "vl"), rest[14:18]))
+    ends = [(h, way) for h in "gv" for way in (1, -1)]
+    LAND, SUMS = dict(zip(ends, rest[10:14])), dict(zip(ends, rest[14:18]))
     IP, IR, IS, ISR = parts_of(XB, [2 * NX, NX, NX, 3])
     TY, TZ1, TB, TT = parts_of(TS, [4, 4, 4, 8])
     rep, fs, tp = lax.axis_index("rep"), lax.axis_index("fs"), lax.axis_index("tp")
@@ -249,13 +249,13 @@
     value_z(1)
     gate_y(1)
     gate_y(3)
-    edges_spread()
     gate_y(2)
     gate_z(0, 1)
     value_y(0)
     value_z(2)
     gate_z(3, 1)
     gate_z(1, 1)
+    edges_spread()
     gate_z(2, 1)
     value_y(1)
     value_y(-1)
@@ -370,8 +370,8 @@
     place = {dz % ZL: k for k, dz in enumerate(order)}
     COT, TERMS = {"g": CG, "v": CV}, {"g": GG, "v": GV}
 
-    def turn(k):
-        return (1, up, down) if k % 2 == 0 else (-1, down, up)
+    def turn(h, k):
+        return (1, up, down) if (k % 2 == 0) == (h == "g") else (-1, down, up)
 
     def make_blocks(h, k):
         dz = order[k]
@@ -381,7 +381,7 @@
             (((0,), (0,)), ((), ())), preferred_element_type=F32,
         )
         TERMS[h][pl.ds(z * NY, NY)] = block.astype(BF16).reshape(NY, 64, COLS)
-        way, onward, back = turn(k)
+        way, onward, back = turn(h, k)
         w.send(("far", h, k), TERMS[h].at[blk(dz, 2)], FAR[h].at[k], onward)
         w.send(("dir", h, k), TERMS[h].at[blk(dz, -way)], DIR[h].at[k], back)
 
@@ -392,7 +392,7 @@
         return acc
 
     def pass_on(h, k):
-        way, onward, back = turn(k)
+        way, onward, back = turn(h, k)
         w.wait(("far", h, k), FAR[h].at[k], me)
         MID[h][k] = total(FAR[h][k], TERMS[h][blk(order[k], way)]).astype(BF16)
         w.send(("mid", h, k), MID[h].at[k], END[h].at[k], onward)
@@ -402,33 +402,30 @@
         w.wait(("mid", h, k), END[h].at[k], me)
         RED[h][k] = total(TERMS[h][blk(order[k], 0)], DIR[h][k], END[h][k]).astype(BF16)
 
-    chains = {
-        "gr": ("g", ZRG, -1, 0, 8, right, None),
-        "gl": ("g", ZLG, 1, 1, 7, left, None),
-        "vr": ("v", ZRV, -1, 1, 7, right, dev(z=zg + 4)),
-        "vl": ("v", ZLV, 1, 0, 8, left, dev(z=zg - 4)),
-    }
-
-    def hop(name, s):
-        h, landing, way, start, length, to, end = chains[name]
-        k = place[(way * (start + s)) % ZL]
-        cut = length - 4 if end is not None else None
-        first = s == 0 or (cut is not None and s == cut + 1)
-        slot = landing.at[s]
-        if first:
-            w.send((name, s), RED[h].at[k], slot, to)
-            return
-        w.wait((name, s - 1), landing.at[s - 1], me)
-        SUMS[name][s] = total(landing[s - 1], RED[h][k]).astype(BF16)
-        w.send((name, s), SUMS[name].at[s], slot, end if s == cut else to)
-
-    def finish(h, names, out):
+    def start_of(h, way):
+        return 8 if (h == "g") == (way == 1) else 7
+
+    def row_at(way, d):
+        return place[(way * d) % ZL]
+
+    def hop(h, way, d):
+        landing = LAND[h, way]
+        k = row_at(way, d)
+        if d in (start_of(h, way), 3, 2):
+            source = RED[h].at[k]
+        else:
+            w.wait((h, way, d), landing.at[d], me)
+            SUMS[h, way][d] = total(landing[d], RED[h][k]).astype(BF16)
+            source = SUMS[h, way].at[d]
+        slot, to = (d - 1, 1) if d not in (3, 4) else (d - 1, d)
+        w.send((h, way, slot), source, landing.at[slot], dev(z=zg + way * to))
+
+    def finish(h, out):
         parts = [RED[h][place[0]]]
-        for name in names:
-            _, landing, _, _, length, _, end = chains[name]
-            for s in (length - 1,) if end is None else (length - 1, length - 4):
-                w.wait((name, s), landing.at[s], me)
-                parts.append(landing[s])
+        for way in (1, -1):
+            for slot in (0, 2, 3):
+                w.wait((h, way, slot), LAND[h, way].at[slot], me)
+                parts.append(LAND[h, way][slot])
         out[...] = total(*parts) * factor
 
     def input_terms(j):
@@ -495,49 +492,43 @@
         w.wait(("tt",), TT.at[pl.ds(0, 7)], me, "taps")
         put_out(TT, tout_hbm)
 
-    steps = [(h, k) for h in "gv" for k in range(ZL)]
-    after_row = {
-        ("g", 0): [("gr", 0)],
-        ("g", 1): [("gl", 0)],
-        ("g", 2): [("gr", 1)],
-        ("g", 3): [("gl", 1)],
-        ("g", 4): [("gr", 2)],
-        ("g", 5): [("gl", 2)],
-        ("g", 6): [("gr", 3)],
-        ("g", 7): [("gl", 3), ("gr", 4)],
-        ("v", 0): [("vl", 0)],
-        ("v", 1): [("vl", 1), ("gl", 4), ("gr", 5)],
-        ("v", 2): [("vr", 0)],
-        ("v", 3): [("vl", 2), ("gl", 5), ("gr", 6)],
-        ("v", 4): [("vr", 1)],
-        ("v", 5): [("vl", 3), ("vr", 4)],
-        ("v", 6): [("vr", 2), ("vl", 5), ("gl", 6), ("gr", 7)],
-        ("v", 7): [("vl", 4), ("vr", 3)],
-    }
-    extra = {2: [taps_y], 6: [taps_z], 10: [lambda: taps_pair(0)], 11: [input_swap], 13: [lambda: taps_pair(1)],
-             14: [input_sums], 16: [taps_spread]}
-    for j in range(8):
-        extra.setdefault(3 + j, []).append(functools.partial(input_terms, j))
-    for i in range(len(steps) + 5):
-        if i < len(steps):
-            make_blocks(*steps[i])
-        if 0 <= i - 3 < len(steps):
-            pass_on(*steps[i - 3])
-        if 0 <= i - 5 < len(steps):
-            row_done(*steps[i - 5])
-            for name, s in after_row[steps[i - 5]]:
-                hop(name, s)
-        for run in extra.get(i, ()):
+    items = [(h, k) for k in range(5) for h in "gv"]
+    items += [(h, k) for h in "gv" for k in (5, 6, 7)]
+    ahead, lag, spacing = 4, 3, 3
+    row_step = {item: t + lag for t, item in enumerate(items)}
+    hop_step = {}
+    for h, way in ends:
+        for d in range(start_of(h, way), 0, -1):
+            step = row_step[h, row_at(way, d)]
+            if (h, way, d + 1) in hop_step and d not in (3, 2):
+                step = max(step, hop_step[h, way, d + 1] + spacing)
+            hop_step[h, way, d] = step
+    extra = {4: [taps_z], 5: [input_swap], 8: [lambda: taps_pair(0)], 9: [input_sums], 12: [lambda: taps_pair(1)],
+             16: [taps_spread]}
+    for j in range(4, 8):
+        extra.setdefault(j - 3, []).insert(0, functools.partial(input_terms, j))
+    for item in items[:ahead]:
+        make_blocks(*item)
+    taps_y()
+    for j in range(4):
+        input_terms(j)
+    for step in range(max(hop_step.values()) + 1):
+        if step < len(items):
+            pass_on(*items[step])
+        if step + ahead < len(items):
+            make_blocks(*items[step + ahead])
+        if 0 <= step - lag < len(items):
+            row_done(*items[step - lag])
+        for key in sorted(hop_step, key=hop_step.get):
+            if hop_step[key] == step:
+                hop(*key)
+        for run in extra.get(step, ()):
             run()
-    hop("vl", 6)
-    hop("vr", 5)
     input_done()
     taps_done()
-    finish("g", ("gr", "gl"), DG)
+    finish("g", DG)
     put_out(DG, dg_hbm)
-    hop("vl", 7)
-    hop("vr", 6)
-    finish("v", ("vl", "vr"), DV)
+    finish("v", DV)
     put_out(DV, dv_hbm)
     w.drain(
         {

time: 95.7 us -> 93.5 us (0.977)
  Pallas kernels: 94.3 us -> 92.1 us
    pallas_call x1, Pallas kernels: 92.5 us -> 90.2 us  [shards(): pl.pallas_call(functools.partial(kernel, factor), out_shape=(tile, grad,...]
where the time goes in v3:
time: 93.5 us; the launch traced here: 92.7 us
  Pallas kernels  92.1 us (99%)
    pallas_call x1, Pallas kernels, shards(): pl.pallas_call(functools.partial(kernel, factor), out_shape=(tile, grad,...  90.2 us

profile of v3, /device:TPU:24, one launch (start us, length us, event | category | flops | bytes accessed | tf_op | source)
XLA Modules:
  0.0 92.7 jit_solution(11324507327107998565)
XLA Ops:
  0.6 90.2 %shard_map.101 = (bf16[384,256]{1,0:T(8,128)(2,1)}, f32[64,352]{1,0:T(8,128)}, f32[64,352]{1,0:T(8,128)}, f32[8,8,352]{2,1,0:T(8,128)}) custom-call(bf16[384,256]{1,0:T(8,128)(2,1)} %bitcast.6, bf16[64,352]{1,0:T(8,128)(2,1)} %wg_hbm.1, bf16[64,352]{1,0:T(8,128)(2,1)} %wv_hbm.1, f32[3,2816]{1,0:T(4,128)} %gt_hbm.1, f32[3,2816]{1,0:T(4,128)} %vt_hbm.1, ...), custom_call_target="tpu_custom_call" | custom-call | tf_op jit(solution)/shard_map/pallas_call | solution.py:593
  90.8 1.9 %shard_map.102 = (bf16[384,256]{1,0:T(8,128)(2,1)}, f32[64,352]{1,0:T(8,128)}, f32[64,352]{1,0:T(8,128)}, f32[3,2816]{1,0:T(4,128)}, f32[3,2816]{1,0:T(4,128)}) custom-call(bf16[384,256]{1,0:T(8,128)(2,1)} %get-tuple-element.14.din_ref, f32[64,352]{1,0:T(8,128)} %get-tuple-element.15.dg_ref, f32[64,352]{1,0:T(8,128)} %get-tuple-element.16.dv_ref, ...), custom_call_target="tpu_custom_call" | custom-call | tf_op jit(solution)/shard_map/pallas_call | solution.py:603

commit v4 on v3

--- a/solution.py
+++ b/solution.py
@@ -129,8 +129,6 @@
     peers = [tp_peer(k) for k in range(1, 8)]
     peers += [dev(y=y + k) for k in (1, 2, 3)]
     peers += [right, left, after, before]
-    peers += [z_near(k) for k in (1, 2, 3)]
-    peers += [dev(z=zg + 4), dev(z=zg - 4)]
     for peer in peers:
         pl.semaphore_signal(barrier, inc=1, device_id=peer, device_id_type=MESH)
     pl.semaphore_wait(barrier, len(peers))
@@ -232,11 +230,13 @@
                     w.send(("vz", way, d + 1), unit, unit, to)
                 w.send(("vy", dz, 1), unit, unit, up)
                 w.send(("vy", dz, -1), unit, unit, down)
+                if d == 4:
+                    w.send(("vf", dz), unit, unit, dev(y=y + 2))
 
     def value_y(dz):
         from_down, from_up = WV.at[blk(dz, -1)], WV.at[blk(dz, 1)]
         w.wait(("vy", dz, 1), from_down, me)
-        if dz % 2 == 0:
+        if dz % 2 == 0 and dz != -4:
             w.send(("vf", dz), from_down, from_down, up)
         w.wait(("vy", dz, -1), from_up, me)
         if dz % 2 == 1:
@@ -405,25 +405,30 @@
     def start_of(h, way):
         return 8 if (h == "g") == (way == 1) else 7
 
+    direct = {"g": {4: (3, 4)}, "v": {5: (4, 5), 4: (3, 4)}}
+    starts = {
+        (h, way): (start_of(h, way), 3) if h == "g" else (start_of(h, way), 4, 3) for h, way in ends
+    }
+
     def row_at(way, d):
         return place[(way * d) % ZL]
 
     def hop(h, way, d):
         landing = LAND[h, way]
         k = row_at(way, d)
-        if d in (start_of(h, way), 3, 2):
+        if d in starts[h, way]:
             source = RED[h].at[k]
         else:
             w.wait((h, way, d), landing.at[d], me)
             SUMS[h, way][d] = total(landing[d], RED[h][k]).astype(BF16)
             source = SUMS[h, way].at[d]
-        slot, to = (d - 1, 1) if d not in (3, 4) else (d - 1, d)
+        slot, to = direct[h].get(d, (d - 1, 1))
         w.send((h, way, slot), source, landing.at[slot], dev(z=zg + way * to))
 
     def finish(h, out):
         parts = [RED[h][place[0]]]
         for way in (1, -1):
-            for slot in (0, 2, 3):
+            for slot in [0] + [slot for slot, _ in direct[h].values()]:
                 w.wait((h, way, slot), LAND[h, way].at[slot], me)
                 parts.append(LAND[h, way][slot])
         out[...] = total(*parts) * factor
@@ -492,19 +497,18 @@
         w.wait(("tt",), TT.at[pl.ds(0, 7)], me, "taps")
         put_out(TT, tout_hbm)
 
-    items = [(h, k) for k in range(5) for h in "gv"]
-    items += [(h, k) for h in "gv" for k in (5, 6, 7)]
+    items = [("v", k) for k in range(3)] + [("g", k) for k in range(ZL)] + [("v", k) for k in range(3, ZL)]
     ahead, lag, spacing = 4, 3, 3
     row_step = {item: t + lag for t, item in enumerate(items)}
     hop_step = {}
     for h, way in ends:
         for d in range(start_of(h, way), 0, -1):
             step = row_step[h, row_at(way, d)]
-            if (h, way, d + 1) in hop_step and d not in (3, 2):
+            if d not in starts[h, way]:
                 step = max(step, hop_step[h, way, d + 1] + spacing)
             hop_step[h, way, d] = step
-    extra = {4: [taps_z], 5: [input_swap], 8: [lambda: taps_pair(0)], 9: [input_sums], 12: [lambda: taps_pair(1)],
-             16: [taps_spread]}
+    extra = {4: [taps_z], 5: [input_swap], 8: [lambda: taps_pair(0)], 9: [input_sums], 13: [lambda: taps_pair(1)],
+             19: [taps_spread]}
     for j in range(4, 8):
         extra.setdefault(j - 3, []).insert(0, functools.partial(input_terms, j))
     for item in items[:ahead]:

time: 93.5 us -> 96.2 us (1.029)
  Pallas kernels: 92.1 us -> 94.8 us
    pallas_call x1, Pallas kernels: 90.2 us -> 92.9 us  [shards(): pl.pallas_call(functools.partial(kernel, factor), out_shape=(tile, grad,...]
where the time goes in v4:
time: 96.2 us; the launch traced here: 95.4 us
  Pallas kernels  94.8 us (99%)
    pallas_call x1, Pallas kernels, shards(): pl.pallas_call(functools.partial(kernel, factor), out_shape=(tile, grad,...  92.9 us

profile of v4, /device:TPU:24, one launch (start us, length us, event | category | flops | bytes accessed | tf_op | source)
XLA Modules:
  0.0 95.4 jit_solution(9511481867872005436)
XLA Ops:
  0.6 92.9 %shard_map.101 = (bf16[384,256]{1,0:T(8,128)(2,1)}, f32[64,352]{1,0:T(8,128)}, f32[64,352]{1,0:T(8,128)}, f32[8,8,352]{2,1,0:T(8,128)}) custom-call(bf16[384,256]{1,0:T(8,128)(2,1)} %bitcast.6, bf16[64,352]{1,0:T(8,128)(2,1)} %wg_hbm.1, bf16[64,352]{1,0:T(8,128)(2,1)} %wv_hbm.1, f32[3,2816]{1,0:T(4,128)} %gt_hbm.1, f32[3,2816]{1,0:T(4,128)} %vt_hbm.1, ...), custom_call_target="tpu_custom_call" | custom-call | tf_op jit(solution)/shard_map/pallas_call | solution.py:597
  93.6 1.9 %shard_map.102 = (bf16[384,256]{1,0:T(8,128)(2,1)}, f32[64,352]{1,0:T(8,128)}, f32[64,352]{1,0:T(8,128)}, f32[3,2816]{1,0:T(4,128)}, f32[3,2816]{1,0:T(4,128)}) custom-call(bf16[384,256]{1,0:T(8,128)(2,1)} %get-tuple-element.14.din_ref, f32[64,352]{1,0:T(8,128)} %get-tuple-element.15.dg_ref, f32[64,352]{1,0:T(8,128)} %get-tuple-element.16.dv_ref, ...), custom_call_target="tpu_custom_call" | custom-call | tf_op jit(solution)/shard_map/pallas_call | solution.py:607

commit v5 on v4

--- a/solution.py
+++ b/solution.py
@@ -43,8 +43,8 @@
             device_id_type=MESH,
         )
 
-    def send(self, key, src, dst, to, kind="unit"):
-        self.count[kind] += 1
+    def send(self, key, src, dst, to, kind="unit", amount=1):
+        self.count[kind] += amount
         self.copy(key, src, dst, to, kind).start()
 
     def wait(self, key, dst, to, kind="unit"):
@@ -52,7 +52,7 @@
 
     def drain(self, spans, to):
         for kind, span in spans.items():
-            whole = span(self.count[kind])
+            whole = span(int(self.count[kind]))
             self.copy(("drain",), whole, whole, to, kind).wait_send()
 
 
@@ -149,8 +149,14 @@
     w.send(("hx", 1), tail, X.at[tp, lo], after, "edge")
     w.send(("hx", -1), head, X.at[tp, hi], before, "edge")
     mine = X.at[tp, pl.ds(EDGE, TOK)]
-    for dx in (1, 3, 2):
-        w.send(("x", dx), mine, mine, dev(x=x + dx), "tile")
+    HALF = TOK // 2
+
+    def half_of(dx, i):
+        return X.at[lax.rem(x - dx + NX, NX) * NC + c, pl.ds(EDGE + HALF * i, HALF)]
+
+    for i in (0, 1):
+        for way, part in ((1, half_of(0, i)), (-1, half_of(0, 1 - i))):
+            w.send(("x", way, i), part, part, dev(x=x + way), "tile", 0.5)
     w.send(("xp", 0), mine, mine, partner, "tile")
     w.send(("vy", 0, 1), WV.at[own], WV.at[own], up)
     w.send(("vy", 0, -1), WV.at[own], WV.at[own], down)
@@ -165,7 +171,10 @@
                     block.T[:, :cols].astype(BF16)
                 )
 
-    def gate_chunk(z, first=False):
+    def rounded(value):
+        return value.astype(BF16).astype(F32)
+
+    def gate_chunk(z, first=False, last=False):
         part = jnp.dot(
             X[z],
             WG[pl.ds(z * NY, NY)].reshape(FEAT, COLS),
@@ -173,10 +182,12 @@
         )
         if first:
             PG[8 : 8 + EXT] = part
+        elif last:
+            PG[8 : 8 + EXT] = rounded(PG[8 : 8 + EXT] + part)
         else:
             PG[8 : 8 + EXT] += part
 
-    def value_chunk(z, first=False):
+    def value_chunk(z, first=False, last=False):
         part = jnp.dot(
             X[z],
             WV[pl.ds(z * NY, NY)].reshape(FEAT, COLS),
@@ -184,13 +195,30 @@
         )
         if first:
             PV[8 : 8 + EXT] = part
+        elif last:
+            PV[8 : 8 + EXT] = rounded(PV[8 : 8 + EXT] + part)
         else:
             PV[8 : 8 + EXT] += part
 
-    def x_arrived(dx):
+    def x_first():
+        for way in (1, -1):
+            part = half_of(way, (1 - way) // 2)
+            w.wait(("x", way, 0), part, me, "tile")
+            w.send(("x2", way), part, part, dev(x=x + way), "tile", 0.5)
+
+    def x_whole(dx):
         slot = X.at[lax.rem(x - dx + NX, NX) * NC + c, pl.ds(EDGE, TOK)]
-        w.wait(("x", dx), slot, me, "tile")
         w.send(("xp", dx), slot, slot, partner, "tile")
+
+    def x_near():
+        for way in (1, -1):
+            w.wait(("x", way, 1), half_of(way, (1 + way) // 2), me, "tile")
+            x_whole(way)
+
+    def x_far():
+        for way in (1, -1):
+            w.wait(("x2", way), half_of(2, (1 - way) // 2), me, "tile")
+        x_whole(2)
 
     def xp_arrived(dx):
         slot = X.at[lax.rem(x - dx + NX, NX) * NC + 1 - c, pl.ds(EDGE, TOK)]
@@ -242,9 +270,9 @@
         if dz % 2 == 1:
             w.send(("vf", dz), from_up, from_up, down)
 
-    def value_row(dz, first=False):
+    def value_row(dz, first=False, last=False):
         w.wait(("vf", dz), WV.at[blk(dz, 2)], me)
-        value_chunk(zrow(dz), first)
+        value_chunk(zrow(dz), first, last)
 
     value_z(1)
     gate_y(1)
@@ -254,55 +282,55 @@
     value_y(0)
     value_z(2)
     gate_z(3, 1)
+    x_first()
     gate_z(1, 1)
     edges_spread()
     gate_z(2, 1)
     value_y(1)
     value_y(-1)
+    x_near()
     out_grad_rows()
     gate_z(0, 2)
     value_z(3)
     w.send(("og", 1), OG.at[pl.ds(TOK, EDGE)], OG.at[lo], after, "og")
     w.send(("og", -1), OG.at[pl.ds(EDGE, EDGE)], OG.at[hi], before, "og")
-    x_arrived(1)
-    x_arrived(3)
     gate_z(3, 2)
     value_y(2)
     value_y(-2)
     gate_z(1, 2)
+    x_far()
     gate_z(2, 2)
     gate_z(0, 3)
     value_z(4)
-    x_arrived(2)
-    gate_z(3, 3)
-    value_y(3)
-    value_y(-3)
-    gate_z(1, 3)
-    for dx in (0, 1, 3, 2):
+    for dx in (0, 1, -1, 2):
         xp_arrived(dx)
     edges_done()
     gate_chunk(zrow(0), first=True)
     gate_chunk(zrow(1))
+    gate_z(3, 3)
+    gate_chunk(zrow(-1))
+    value_y(3)
+    value_y(-3)
+    gate_z(1, 3)
+    value_row(0, first=True)
+    gate_chunk(zrow(2))
     gate_z(2, 3)
-    gate_chunk(zrow(-1))
-    value_row(0, first=True)
+    gate_chunk(zrow(-2))
+    value_row(1)
     gate_z(0, 4)
-    gate_chunk(zrow(2))
-    gate_chunk(zrow(-2))
+    value_row(-1)
+    value_row(2)
+    gate_chunk(zrow(3))
+    gate_z(3, 4)
+    value_row(-2)
+    gate_chunk(zrow(-3))
     value_y(-4)
-    gate_z(3, 4)
-    value_row(1)
-    value_row(-1)
+    value_row(3)
     gate_z(1, 4)
-    value_row(2)
-    value_row(-2)
+    value_row(-3)
+    value_row(-4, last=True)
     gate_z(2, 4)
-    gate_chunk(zrow(3))
-    gate_chunk(zrow(-3))
-    gate_chunk(zrow(4))
-    value_row(3)
-    value_row(-3)
-    value_row(-4)
+    gate_chunk(zrow(4), last=True)
     w.wait(("og", 1), OG.at[lo], me, "og")
     w.wait(("og", -1), OG.at[hi], me, "og")
 
@@ -319,13 +347,10 @@
     taps = pltpu.roll(taps, lax.rem((8 - tp) * COLS, 8 * COLS), axis=1)[:, :COLS]
     g0, g1, g2, v0, v1, v2 = (taps[k : k + 1] for k in range(6))
 
-    def rounded(value):
-        return value.astype(BF16).astype(F32)
-
     def cot_rows(i):
         base = pl.multiple_of(i * 16, 16)
-        gate = rounded(PG[pl.ds(base, 32)])
-        value = rounded(PV[pl.ds(base, 32)])
+        gate = PG[pl.ds(base, 32)]
+        value = PV[pl.ds(base, 32)]
         gm, gz, gp = gate[7:23], gate[8:24], gate[9:25]
         vm, vz, vp = value[7:23], value[8:24], value[9:25]
         gate_mix = g0 * gm + g1 * gz + g2 * gp
@@ -405,10 +430,8 @@
     def start_of(h, way):
         return 8 if (h == "g") == (way == 1) else 7
 
-    direct = {"g": {4: (3, 4)}, "v": {5: (4, 5), 4: (3, 4)}}
-    starts = {
-        (h, way): (start_of(h, way), 3) if h == "g" else (start_of(h, way), 4, 3) for h, way in ends
-    }
+    direct = {4: (3, 4)}
+    starts = {(h, way): (start_of(h, way), 3) for h, way in ends}
 
     def row_at(way, d):
         return place[(way * d) % ZL]
@@ -422,13 +445,13 @@
             w.wait((h, way, d), landing.at[d], me)
             SUMS[h, way][d] = total(landing[d], RED[h][k]).astype(BF16)
             source = SUMS[h, way].at[d]
-        slot, to = direct[h].get(d, (d - 1, 1))
+        slot, to = direct.get(d, (d - 1, 1))
         w.send((h, way, slot), source, landing.at[slot], dev(z=zg + way * to))
 
     def finish(h, out):
         parts = [RED[h][place[0]]]
         for way in (1, -1):
-            for slot in [0] + [slot for slot, _ in direct[h].values()]:
+            for slot in [0] + [slot for slot, _ in direct.values()]:
                 w.wait((h, way, slot), LAND[h, way].at[slot], me)
                 parts.append(LAND[h, way][slot])
         out[...] = total(*parts) * factor
@@ -497,7 +520,8 @@
         w.wait(("tt",), TT.at[pl.ds(0, 7)], me, "taps")
         put_out(TT, tout_hbm)
 
-    items = [("v", k) for k in range(3)] + [("g", k) for k in range(ZL)] + [("v", k) for k in range(3, ZL)]
+    items = [(h, k) for k in range(5) for h in "gv"]
+    items += [(h, k) for h in "gv" for k in (5, 6, 7)]
     ahead, lag, spacing = 4, 3, 3
     row_step = {item: t + lag for t, item in enumerate(items)}
     hop_step = {}
@@ -550,7 +574,7 @@
         raise ValueError(str(len(w.index)))
 
 
-RECEIVES = 165
+RECEIVES = 168
 
 
 def finisher(din_ref, dg_ref, dv_ref, tt_ref, din_out, dg_out, dv_out, tg_out, tv_out):

time: 96.2 us -> 89.9 us (0.935)
  Pallas kernels: 94.8 us -> 89 us
    pallas_call x1, Pallas kernels: 92.9 us -> 87.2 us  [shards(): pl.pallas_call(functools.partial(kernel, factor), out_shape=(tile, grad,...]
where the time goes in v5:
time: 89.9 us; the launch traced here: 89.7 us
  Pallas kernels  89 us (99%)
    pallas_call x1, Pallas kernels, shards(): pl.pallas_call(functools.partial(kernel, factor), out_shape=(tile, grad,...  87.2 us
    pallas_call x1, Pallas kernels, shards(): pl.pallas_call(finisher, out_shape=(tile, grad, grad, tap, tap), in_specs...  1.86 us

profile of v5, /device:TPU:24, one launch (start us, length us, event | category | flops | bytes accessed | tf_op | source)
XLA Modules:
  0.0 89.7 jit_solution(442257003082039928)
XLA Ops:
  0.6 87.2 %shard_map.101 = (bf16[384,256]{1,0:T(8,128)(2,1)}, f32[64,352]{1,0:T(8,128)}, f32[64,352]{1,0:T(8,128)}, f32[8,8,352]{2,1,0:T(8,128)}) custom-call(bf16[384,256]{1,0:T(8,128)(2,1)} %bitcast.6, bf16[64,352]{1,0:T(8,128)(2,1)} %wg_hbm.1, bf16[64,352]{1,0:T(8,128)(2,1)} %wv_hbm.1, f32[3,2816]{1,0:T(4,128)} %gt_hbm.1, f32[3,2816]{1,0:T(4,128)} %vt_hbm.1, ...), custom_call_target="tpu_custom_call" | custom-call | tf_op jit(solution)/shard_map/pallas_call | solution.py:621
  87.8 1.9 %shard_map.102 = (bf16[384,256]{1,0:T(8,128)(2,1)}, f32[64,352]{1,0:T(8,128)}, f32[64,352]{1,0:T(8,128)}, f32[3,2816]{1,0:T(4,128)}, f32[3,2816]{1,0:T(4,128)}) custom-call(bf16[384,256]{1,0:T(8,128)(2,1)} %get-tuple-element.14.din_ref, f32[64,352]{1,0:T(8,128)} %get-tuple-element.15.dg_ref, f32[64,352]{1,0:T(8,128)} %get-tuple-element.16.dv_ref, ...), custom_call_target="tpu_custom_call" | custom-call | tf_op jit(solution)/shard_map/pallas_call | solution.py:631

commit v6 on v5

--- a/solution.py
+++ b/solution.py
@@ -292,13 +292,13 @@
     out_grad_rows()
     gate_z(0, 2)
     value_z(3)
+    x_far()
     w.send(("og", 1), OG.at[pl.ds(TOK, EDGE)], OG.at[lo], after, "og")
     w.send(("og", -1), OG.at[pl.ds(EDGE, EDGE)], OG.at[hi], before, "og")
     gate_z(3, 2)
     value_y(2)
     value_y(-2)
     gate_z(1, 2)
-    x_far()
     gate_z(2, 2)
     gate_z(0, 3)
     value_z(4)
@@ -522,7 +522,7 @@
 
     items = [(h, k) for k in range(5) for h in "gv"]
     items += [(h, k) for h in "gv" for k in (5, 6, 7)]
-    ahead, lag, spacing = 4, 3, 3
+    ahead, lag, spacing = 6, 3, 3
     row_step = {item: t + lag for t, item in enumerate(items)}
     hop_step = {}
     for h, way in ends:
@@ -531,6 +531,17 @@
             if d not in starts[h, way]:
                 step = max(step, hop_step[h, way, d + 1] + spacing)
             hop_step[h, way, d] = step
+    late = {
+        16: [("v", 1, 3), ("v", -1, 5), ("g", -1, 4)],
+        17: [("v", -1, 3), ("v", 1, 5), ("g", 1, 4)],
+        18: [("g", 1, 2), ("g", -1, 2), ("v", -1, 4), ("v", 1, 4)],
+        19: [("g", 1, 1), ("v", 1, 2), ("g", -1, 1), ("v", -1, 2)],
+        20: [("v", 1, 1), ("v", -1, 1)],
+    }
+    for step, keys in late.items():
+        for key in keys:
+            del hop_step[key]
+            hop_step[key] = step
     extra = {4: [taps_z], 5: [input_swap], 8: [lambda: taps_pair(0)], 9: [input_sums], 13: [lambda: taps_pair(1)],
              19: [taps_spread]}
     for j in range(4, 8):

time: 89.9 us -> 91.2 us (1.014)
  no operation moved by 1% of the time
where the time goes in v6:
time: 91.2 us; the launch traced here: 90.5 us
  Pallas kernels  89.9 us (99%)
    pallas_call x1, Pallas kernels, shards(): pl.pallas_call(functools.partial(kernel, factor), out_shape=(tile, grad,...  88 us
    pallas_call x1, Pallas kernels, shards(): pl.pallas_call(finisher, out_shape=(tile, grad, grad, tap, tap), in_specs...  1.86 us

profile of v6, /device:TPU:24, one launch (start us, length us, event | category | flops | bytes accessed | tf_op | source)
XLA Modules:
  0.0 90.5 jit_solution(6445486631293739262)
XLA Ops:
  0.6 88.0 %shard_map.101 = (bf16[384,256]{1,0:T(8,128)(2,1)}, f32[64,352]{1,0:T(8,128)}, f32[64,352]{1,0:T(8,128)}, f32[8,8,352]{2,1,0:T(8,128)}) custom-call(bf16[384,256]{1,0:T(8,128)(2,1)} %bitcast.6, bf16[64,352]{1,0:T(8,128)(2,1)} %wg_hbm.1, bf16[64,352]{1,0:T(8,128)(2,1)} %wv_hbm.1, f32[3,2816]{1,0:T(4,128)} %gt_hbm.1, f32[3,2816]{1,0:T(4,128)} %vt_hbm.1, ...), custom_call_target="tpu_custom_call" | custom-call | tf_op jit(solution)/shard_map/pallas_call | solution.py:632
  88.7 1.9 %shard_map.102 = (bf16[384,256]{1,0:T(8,128)(2,1)}, f32[64,352]{1,0:T(8,128)}, f32[64,352]{1,0:T(8,128)}, f32[3,2816]{1,0:T(4,128)}, f32[3,2816]{1,0:T(4,128)}) custom-call(bf16[384,256]{1,0:T(8,128)(2,1)} %get-tuple-element.14.din_ref, f32[64,352]{1,0:T(8,128)} %get-tuple-element.15.dg_ref, f32[64,352]{1,0:T(8,128)} %get-tuple-element.16.dv_ref, ...), custom_call_target="tpu_custom_call" | custom-call | tf_op jit(solution)/shard_map/pallas_call | solution.py:642

commit v7 on v5

--- a/solution.py
+++ b/solution.py
@@ -22,6 +22,14 @@
 
 def right_reach(r):
     return 4 if r < 2 else 3
+
+
+TREES = {
+    "g": {8: 7, 7: 6, 6: 5, 5: 4, 4: 3, 3: 2, 2: 1, 1: 0},
+    "v": {8: 7, 7: 6, 6: 5, 5: 4, 4: 0, 3: 2, 2: 1, 1: 0},
+}
+ITEMS = [(h, k) for h in "gv" for k in range(ZL)]
+AHEAD, SPACING = 4, 3
 
 
 class Wires:
@@ -70,7 +78,7 @@
             first += size
         return parts
 
-    WG, WV, GG, GV, *rest = parts_of(U, [32] * 4 + [8] * 18)
+    WG, WV, GG, GV, *rest = parts_of(U, [32] * 4 + [8] * 10 + [9] * 8)
     FAR, DIR, MID, END, RED = ({"g": rest[2 * i], "v": rest[2 * i + 1]} for i in range(5))
     ends = [(h, way) for h in "gv" for way in (1, -1)]
     LAND, SUMS = dict(zip(ends, rest[10:14])), dict(zip(ends, rest[14:18]))
@@ -292,13 +300,13 @@
     out_grad_rows()
     gate_z(0, 2)
     value_z(3)
+    x_far()
     w.send(("og", 1), OG.at[pl.ds(TOK, EDGE)], OG.at[lo], after, "og")
     w.send(("og", -1), OG.at[pl.ds(EDGE, EDGE)], OG.at[hi], before, "og")
     gate_z(3, 2)
     value_y(2)
     value_y(-2)
     gate_z(1, 2)
-    x_far()
     gate_z(2, 2)
     gate_z(0, 3)
     value_z(4)
@@ -430,31 +438,29 @@
     def start_of(h, way):
         return 8 if (h == "g") == (way == 1) else 7
 
-    direct = {4: (3, 4)}
-    starts = {(h, way): (start_of(h, way), 3) for h, way in ends}
-
     def row_at(way, d):
         return place[(way * d) % ZL]
 
+    def sources(h, way, d):
+        return [e for e in range(start_of(h, way), d, -1) if TREES[h][e] == d]
+
+    def arrived(h, way, d):
+        landing = LAND[h, way]
+        for e in sources(h, way, d):
+            w.wait((h, way, e), landing.at[e], me)
+        return [landing[e] for e in sources(h, way, d)]
+
     def hop(h, way, d):
-        landing = LAND[h, way]
         k = row_at(way, d)
-        if d in starts[h, way]:
-            source = RED[h].at[k]
-        else:
-            w.wait((h, way, d), landing.at[d], me)
-            SUMS[h, way][d] = total(landing[d], RED[h][k]).astype(BF16)
+        source = RED[h].at[k]
+        if sources(h, way, d):
+            SUMS[h, way][d] = total(*arrived(h, way, d), RED[h][k]).astype(BF16)
             source = SUMS[h, way].at[d]
-        slot, to = direct.get(d, (d - 1, 1))
-        w.send((h, way, slot), source, landing.at[slot], dev(z=zg + way * to))
+        w.send((h, way, d), source, LAND[h, way].at[d], dev(z=zg + way * (d - TREES[h][d])))
 
     def finish(h, out):
-        parts = [RED[h][place[0]]]
-        for way in (1, -1):
-            for slot in [0] + [slot for slot, _ in direct.values()]:
-                w.wait((h, way, slot), LAND[h, way].at[slot], me)
-                parts.append(LAND[h, way][slot])
-        out[...] = total(*parts) * factor
+        parts = arrived(h, 1, 0) + arrived(h, -1, 0)
+        out[...] = total(RED[h][place[0]], *parts) * factor
 
     def input_terms(j):
         part = lax.dot_general(
@@ -520,17 +526,14 @@
         w.wait(("tt",), TT.at[pl.ds(0, 7)], me, "taps")
         put_out(TT, tout_hbm)
 
-    items = [(h, k) for k in range(5) for h in "gv"]
-    items += [(h, k) for h in "gv" for k in (5, 6, 7)]
-    ahead, lag, spacing = 4, 3, 3
-    row_step = {item: t + lag for t, item in enumerate(items)}
+    ahead, lag, spacing = AHEAD, 3, SPACING
+    row_step = {item: t + lag for t, item in enumerate(ITEMS)}
     hop_step = {}
     for h, way in ends:
         for d in range(start_of(h, way), 0, -1):
-            step = row_step[h, row_at(way, d)]
-            if d not in starts[h, way]:
-                step = max(step, hop_step[h, way, d + 1] + spacing)
-            hop_step[h, way, d] = step
+            steps = [hop_step[h, way, e] + spacing + e - d - 1 for e in sources(h, way, d)]
+            hop_step[h, way, d] = max([row_step[h, row_at(way, d)], *steps])
+    items = ITEMS
     extra = {4: [taps_z], 5: [input_swap], 8: [lambda: taps_pair(0)], 9: [input_sums], 13: [lambda: taps_pair(1)],
              19: [taps_spread]}
     for j in range(4, 8):
@@ -570,7 +573,7 @@
     )
     for copy in results:
         copy.wait()
-    if len(w.index) != RECEIVES:
+    if len(w.index) > RECEIVES:
         raise ValueError(str(len(w.index)))
 
 
@@ -593,7 +596,7 @@
     vm = pltpu.VMEM
     scratch = [
         vm((8, EXT, FEAT), BF16),
-        vm((272, *unit), BF16),
+        vm((280, *unit), BF16),
         vm((4 * NX + 3, TOK, FEAT), BF16),
         vm((20, 8, cols), F32),
         vm(gate_taps.shape, F32),

time: 89.9 us -> 87.4 us (0.972)
  Pallas kernels: 89 us -> 86.3 us
    pallas_call x1, Pallas kernels: 87.2 us -> 84.5 us  [shards(): pl.pallas_call(functools.partial(kernel, factor), out_shape=(tile, grad,...]
where the time goes in v7:
time: 87.4 us; the launch traced here: 87 us
  Pallas kernels  86.3 us (99%)
    pallas_call x1, Pallas kernels, shards(): pl.pallas_call(functools.partial(kernel, factor), out_shape=(tile, grad,...  84.5 us
    pallas_call x1, Pallas kernels, shards(): pl.pallas_call(finisher, out_shape=(tile, grad, grad, tap, tap), in_specs...  1.86 us

profile of v7, /device:TPU:24, one launch (start us, length us, event | category | flops | bytes accessed | tf_op | source)
XLA Modules:
  0.0 87.0 jit_solution(15376672193120551109)
XLA Ops:
  0.6 84.5 %shard_map.101 = (bf16[384,256]{1,0:T(8,128)(2,1)}, f32[64,352]{1,0:T(8,128)}, f32[64,352]{1,0:T(8,128)}, f32[8,8,352]{2,1,0:T(8,128)}) custom-call(bf16[384,256]{1,0:T(8,128)(2,1)} %bitcast.6, bf16[64,352]{1,0:T(8,128)(2,1)} %wg_hbm.1, bf16[64,352]{1,0:T(8,128)(2,1)} %wv_hbm.1, f32[3,2816]{1,0:T(4,128)} %gt_hbm.1, f32[3,2816]{1,0:T(4,128)} %vt_hbm.1, ...), custom_call_target="tpu_custom_call" | custom-call | tf_op jit(solution)/shard_map/pallas_call | solution.py:624
  85.1 1.9 %shard_map.102 = (bf16[384,256]{1,0:T(8,128)(2,1)}, f32[64,352]{1,0:T(8,128)}, f32[64,352]{1,0:T(8,128)}, f32[3,2816]{1,0:T(4,128)}, f32[3,2816]{1,0:T(4,128)}) custom-call(bf16[384,256]{1,0:T(8,128)(2,1)} %get-tuple-element.14.din_ref, f32[64,352]{1,0:T(8,128)} %get-tuple-element.15.dg_ref, f32[64,352]{1,0:T(8,128)} %get-tuple-element.16.dv_ref, ...), custom_call_target="tpu_custom_call" | custom-call | tf_op jit(solution)/shard_map/pallas_call | solution.py:634

commit v8 on v7

--- a/solution.py
+++ b/solution.py
@@ -18,6 +18,7 @@
 FEAT = 256
 EDGE = 16
 EXT = TOK + 2 * EDGE
+PACK = 176
 
 
 def right_reach(r):
@@ -36,7 +37,7 @@
     def __init__(self, send_sems, recv_sems):
         self.send_sems, self.recv_sems = send_sems, recv_sems
         self.index = {}
-        self.count = dict.fromkeys(("unit", "tile", "edge", "og", "taps"), 0)
+        self.count = dict.fromkeys(("unit", "pack", "tile", "edge", "og", "taps"), 0)
 
     def at(self, key):
         return self.index.setdefault(key, len(self.index))
@@ -68,7 +69,7 @@
     factor,
     x_hbm, wg_hbm, wv_hbm, gt_hbm, vt_hbm, ogt_hbm,
     din_hbm, dg_hbm, dv_hbm, tout_hbm,
-    X, U, XB, TS, GT, VT, OGT, OG, PG, PV, KG, KV, CG, CV, DIN, DG, DV,
+    X, U, Q, XB, TS, GT, VT, OGT, OG, PG, PV, KG, KV, CG, CV, DIN, DG, DV,
     send_sems, recv_sems, local_sems,
 ):
     def parts_of(pool, sizes):
@@ -78,7 +79,8 @@
             first += size
         return parts
 
-    WG, WV, GG, GV, *rest = parts_of(U, [32] * 4 + [8] * 10 + [9] * 8)
+    WG, WV = parts_of(U, [32] * 2)
+    GG, GV, *rest = parts_of(Q, [32] * 2 + [8] * 10 + [9] * 8)
     FAR, DIR, MID, END, RED = ({"g": rest[2 * i], "v": rest[2 * i + 1]} for i in range(5))
     ends = [(h, way) for h in "gv" for way in (1, -1)]
     LAND, SUMS = dict(zip(ends, rest[10:14])), dict(zip(ends, rest[14:18]))
@@ -386,15 +388,16 @@
         (zero,) * 6,
     )
 
-    def back_rows(i, carry):
-        base = pl.multiple_of(i * 16, 16)
-        out = pl.ds(pl.multiple_of(i * 16 - 16, 16), 16)
-        for source, target, (t0, t1, t2) in ((KG, CG, (g0, g1, g2)), (KV, CV, (v0, v1, v2))):
-            cot = source[pl.ds(base, 32)]
+    def back_all(source, target, t0, t1, t2):
+        def back_rows(i, carry):
+            cot = source[pl.ds(pl.multiple_of(i * 16, 16), 32)]
+            out = pl.ds(pl.multiple_of(i * 16 - 16, 16), 16)
             target[out] = (t0 * cot[9:25] + t1 * cot[8:24] + t2 * cot[7:23]).astype(BF16)
-        return carry
-
-    lax.fori_loop(1, TOK // 16 + 1, back_rows, 0)
+            return carry
+
+        lax.fori_loop(1, TOK // 16 + 1, back_rows, 0)
+
+    back_all(KG, CG, g0, g1, g2)
 
     rows = [jnp.sum(part, axis=0, keepdims=True) for part in tap_sums]
     TY[y] = jnp.concatenate(rows + [jnp.zeros((2, COLS), F32)], axis=0)
@@ -405,6 +408,20 @@
 
     def turn(h, k):
         return (1, up, down) if (k % 2 == 0) == (h == "g") else (-1, down, up)
+
+    def packed(block, out):
+        out[0:64] = block[:, :128].astype(BF16)
+        out[64:128] = block[:, 128:256].astype(BF16)
+        rest = block[:, 256:]
+        for j in range(3):
+            row = jnp.concatenate([rest[16 * j : 16 * j + 16], rest[48:64, 32 * j : 32 * j + 32]], axis=1)
+            out[128 + 16 * j : 144 + 16 * j] = row.astype(BF16)
+
+    def unpacked(block, out):
+        out[:, :128] = block[0:64]
+        out[:, 128:256] = block[64:128]
+        last = jnp.concatenate([block[128 + 16 * j : 144 + 16 * j, 96:] for j in range(3)], axis=1)
+        out[:, 256:] = jnp.concatenate([block[128:, :96], last], axis=0)
 
     def make_blocks(h, k):
         dz = order[k]
@@ -413,10 +430,11 @@
             X[z, EDGE : EDGE + TOK, :], COT[h][...],
             (((0,), (0,)), ((), ())), preferred_element_type=F32,
         )
-        TERMS[h][pl.ds(z * NY, NY)] = block.astype(BF16).reshape(NY, 64, COLS)
+        for i in range(NY):
+            packed(block[64 * i : 64 * i + 64], TERMS[h].at[z * NY + i])
         way, onward, back = turn(h, k)
-        w.send(("far", h, k), TERMS[h].at[blk(dz, 2)], FAR[h].at[k], onward)
-        w.send(("dir", h, k), TERMS[h].at[blk(dz, -way)], DIR[h].at[k], back)
+        w.send(("far", h, k), TERMS[h].at[blk(dz, 2)], FAR[h].at[k], onward, "pack")
+        w.send(("dir", h, k), TERMS[h].at[blk(dz, -way)], DIR[h].at[k], back, "pack")
 
     def total(*parts):
         acc = parts[0].astype(F32)
@@ -426,13 +444,13 @@
 
     def pass_on(h, k):
         way, onward, back = turn(h, k)
-        w.wait(("far", h, k), FAR[h].at[k], me)
+        w.wait(("far", h, k), FAR[h].at[k], me, "pack")
         MID[h][k] = total(FAR[h][k], TERMS[h][blk(order[k], way)]).astype(BF16)
-        w.send(("mid", h, k), MID[h].at[k], END[h].at[k], onward)
+        w.send(("mid", h, k), MID[h].at[k], END[h].at[k], onward, "pack")
 
     def row_done(h, k):
-        w.wait(("dir", h, k), DIR[h].at[k], me)
-        w.wait(("mid", h, k), END[h].at[k], me)
+        w.wait(("dir", h, k), DIR[h].at[k], me, "pack")
+        w.wait(("mid", h, k), END[h].at[k], me, "pack")
         RED[h][k] = total(TERMS[h][blk(order[k], 0)], DIR[h][k], END[h][k]).astype(BF16)
 
     def start_of(h, way):
@@ -447,7 +465,7 @@
     def arrived(h, way, d):
         landing = LAND[h, way]
         for e in sources(h, way, d):
-            w.wait((h, way, e), landing.at[e], me)
+            w.wait((h, way, e), landing.at[e], me, "pack")
         return [landing[e] for e in sources(h, way, d)]
 
     def hop(h, way, d):
@@ -456,11 +474,11 @@
         if sources(h, way, d):
             SUMS[h, way][d] = total(*arrived(h, way, d), RED[h][k]).astype(BF16)
             source = SUMS[h, way].at[d]
-        w.send((h, way, d), source, LAND[h, way].at[d], dev(z=zg + way * (d - TREES[h][d])))
+        w.send((h, way, d), source, LAND[h, way].at[d], dev(z=zg + way * (d - TREES[h][d])), "pack")
 
     def finish(h, out):
         parts = arrived(h, 1, 0) + arrived(h, -1, 0)
-        out[...] = total(RED[h][place[0]], *parts) * factor
+        unpacked(total(RED[h][place[0]], *parts) * factor, out)
 
     def input_terms(j):
         part = lax.dot_general(
@@ -541,6 +559,7 @@
     for item in items[:ahead]:
         make_blocks(*item)
     taps_y()
+    back_all(KV, CV, v0, v1, v2)
     for j in range(4):
         input_terms(j)
     for step in range(max(hop_step.values()) + 1):
@@ -564,6 +583,7 @@
     w.drain(
         {
             "unit": lambda n: U.at[pl.ds(0, n)],
+            "pack": lambda n: Q.at[pl.ds(0, n)],
             "tile": lambda n: XB.at[pl.ds(0, n)],
             "edge": lambda n: X.at[0, pl.ds(0, n * EDGE)],
             "og": lambda n: OG.at[pl.ds(0, n * EDGE)],
@@ -596,7 +616,8 @@
     vm = pltpu.VMEM
     scratch = [
         vm((8, EXT, FEAT), BF16),
-        vm((280, *unit), BF16),
+        vm((64, *unit), BF16),
+        vm((216, PACK, 128), BF16),
         vm((4 * NX + 3, TOK, FEAT), BF16),
         vm((20, 8, cols), F32),
         vm(gate_taps.shape, F32),
@@ -612,7 +633,7 @@
         vm((TOK, FEAT), BF16),
         vm(unit, F32),
         vm(unit, F32),
-        pltpu.SemaphoreType.DMA((5,)),
+        pltpu.SemaphoreType.DMA((6,)),
         pltpu.SemaphoreType.DMA((RECEIVES,)),
         pltpu.SemaphoreType.DMA((10,)),
     ]

time: 87.4 us -> 84.7 us (0.969)
  Pallas kernels: 86.3 us -> 83.9 us
    pallas_call x1, Pallas kernels: 84.5 us -> 82 us  [shards(): pl.pallas_call(functools.partial(kernel, factor), out_shape=(tile, grad,...]
where the time goes in v8:
time: 84.7 us; the launch traced here: 84.5 us
  Pallas kernels  83.9 us (99%)
    pallas_call x1, Pallas kernels, shards(): pl.pallas_call(functools.partial(kernel, factor), out_shape=(tile, grad,...  82 us
    pallas_call x1, Pallas kernels, shards(): pl.pallas_call(finisher, out_shape=(tile, grad, grad, tap, tap), in_specs...  1.86 us

profile of v8, /device:TPU:24, one launch (start us, length us, event | category | flops | bytes accessed | tf_op | source)
XLA Modules:
  0.0 84.5 jit_solution(546071396733125827)
XLA Ops:
  0.6 82.0 %shard_map.101 = (bf16[384,256]{1,0:T(8,128)(2,1)}, f32[64,352]{1,0:T(8,128)}, f32[64,352]{1,0:T(8,128)}, f32[8,8,352]{2,1,0:T(8,128)}) custom-call(bf16[384,256]{1,0:T(8,128)(2,1)} %bitcast.6, bf16[64,352]{1,0:T(8,128)(2,1)} %wg_hbm.1, bf16[64,352]{1,0:T(8,128)(2,1)} %wv_hbm.1, f32[3,2816]{1,0:T(4,128)} %gt_hbm.1, f32[3,2816]{1,0:T(4,128)} %vt_hbm.1, ...), custom_call_target="tpu_custom_call" | custom-call | tf_op jit(solution)/shard_map/pallas_call | solution.py:645
  82.7 1.9 %shard_map.102 = (bf16[384,256]{1,0:T(8,128)(2,1)}, f32[64,352]{1,0:T(8,128)}, f32[64,352]{1,0:T(8,128)}, f32[3,2816]{1,0:T(4,128)}, f32[3,2816]{1,0:T(4,128)}) custom-call(bf16[384,256]{1,0:T(8,128)(2,1)} %get-tuple-element.14.din_ref, f32[64,352]{1,0:T(8,128)} %get-tuple-element.15.dg_ref, f32[64,352]{1,0:T(8,128)} %get-tuple-element.16.dv_ref, ...), custom_call_target="tpu_custom_call" | custom-call | tf_op jit(solution)/shard_map/pallas_call | solution.py:655

commit v9 on v8

--- a/solution.py
+++ b/solution.py
@@ -371,22 +371,25 @@
         value_cot = grad * (gate_mix * s)
         KG[pl.ds(base + 8, 16)] = gate_cot
         KV[pl.ds(base + 8, 16)] = value_cot
-        return [
-            (p * k).reshape(2, 8, COLS).sum(axis=0)
-            for p, k in (
-                (gm, gate_cot), (gz, gate_cot), (gp, gate_cot),
-                (vm, value_cot), (vz, value_cot), (vp, value_cot),
-            )
-        ]
-
-    cot_rows(0)
-    cot_rows(TOK // 16 + 1)
-    zero = jnp.zeros((8, COLS), F32)
-    tap_sums = lax.fori_loop(
-        1, TOK // 16 + 1,
-        lambda i, sums: tuple(a + b for a, b in zip(sums, cot_rows(i))),
-        (zero,) * 6,
-    )
+
+    def all_cots(i, carry):
+        cot_rows(i)
+        return carry
+
+    lax.fori_loop(0, TOK // 16 + 2, all_cots, 0)
+
+    def tap_rows(i, sums):
+        base = pl.multiple_of(i * 16, 16)
+        terms = []
+        for pre, cot in ((PG, KG), (PV, KV)):
+            rows, cots = pre[pl.ds(base, 32)], cot[pl.ds(base + 8, 16)]
+            terms += [(rows[7 + k : 23 + k] * cots).reshape(2, 8, COLS).sum(axis=0) for k in range(3)]
+        return tuple(a + b for a, b in zip(sums, terms))
+
+    def taps_own():
+        sums = lax.fori_loop(1, TOK // 16 + 1, tap_rows, (jnp.zeros((8, COLS), F32),) * 6)
+        rows = [jnp.sum(part, axis=0, keepdims=True) for part in sums]
+        TY[y] = jnp.concatenate(rows + [jnp.zeros((2, COLS), F32)], axis=0)
 
     def back_all(source, target, t0, t1, t2):
         def back_rows(i, carry):
@@ -398,9 +401,6 @@
         lax.fori_loop(1, TOK // 16 + 1, back_rows, 0)
 
     back_all(KG, CG, g0, g1, g2)
-
-    rows = [jnp.sum(part, axis=0, keepdims=True) for part in tap_sums]
-    TY[y] = jnp.concatenate(rows + [jnp.zeros((2, COLS), F32)], axis=0)
 
     order = (0, 1, -1, 2, -2, 3, -3, 4)
     place = {dz % ZL: k for k, dz in enumerate(order)}
@@ -552,15 +552,16 @@
             steps = [hop_step[h, way, e] + spacing + e - d - 1 for e in sources(h, way, d)]
             hop_step[h, way, d] = max([row_step[h, row_at(way, d)], *steps])
     items = ITEMS
-    extra = {4: [taps_z], 5: [input_swap], 8: [lambda: taps_pair(0)], 9: [input_sums], 13: [lambda: taps_pair(1)],
+    extra = {4: [taps_z], 7: [input_swap], 8: [lambda: taps_pair(0)], 11: [input_sums], 13: [lambda: taps_pair(1)],
              19: [taps_spread]}
-    for j in range(4, 8):
-        extra.setdefault(j - 3, []).insert(0, functools.partial(input_terms, j))
+    for j in range(2, 8):
+        extra.setdefault(j - 1, []).insert(0, functools.partial(input_terms, j))
     for item in items[:ahead]:
         make_blocks(*item)
+    back_all(KV, CV, v0, v1, v2)
+    taps_own()
     taps_y()
-    back_all(KV, CV, v0, v1, v2)
-    for j in range(4):
+    for j in range(2):
         input_terms(j)
     for step in range(max(hop_step.values()) + 1):
         if step < len(items):

time: 84.7 us -> 84.4 us (level)
  no operation moved by 1% of the time
where the time goes in v9:
time: 84.4 us; the launch traced here: 83.9 us
  Pallas kernels  83.2 us (99%)
    pallas_call x1, Pallas kernels, shards(): pl.pallas_call(functools.partial(kernel, factor), out_shape=(tile, grad,...  81.4 us
    pallas_call x1, Pallas kernels, shards(): pl.pallas_call(finisher, out_shape=(tile, grad, grad, tap, tap), in_specs...  1.86 us

profile of v9, /device:TPU:24, one launch (start us, length us, event | category | flops | bytes accessed | tf_op | source)
XLA Modules:
  0.0 83.9 jit_solution(1448833242545112508)
XLA Ops:
  0.6 81.4 %shard_map.101 = (bf16[384,256]{1,0:T(8,128)(2,1)}, f32[64,352]{1,0:T(8,128)}, f32[64,352]{1,0:T(8,128)}, f32[8,8,352]{2,1,0:T(8,128)}) custom-call(bf16[384,256]{1,0:T(8,128)(2,1)} %bitcast.6, bf16[64,352]{1,0:T(8,128)(2,1)} %wg_hbm.1, bf16[64,352]{1,0:T(8,128)(2,1)} %wv_hbm.1, f32[3,2816]{1,0:T(4,128)} %gt_hbm.1, f32[3,2816]{1,0:T(4,128)} %vt_hbm.1, ...), custom_call_target="tpu_custom_call" | custom-call | tf_op jit(solution)/shard_map/pallas_call | solution.py:646
  82.0 1.9 %shard_map.102 = (bf16[384,256]{1,0:T(8,128)(2,1)}, f32[64,352]{1,0:T(8,128)}, f32[64,352]{1,0:T(8,128)}, f32[3,2816]{1,0:T(4,128)}, f32[3,2816]{1,0:T(4,128)}) custom-call(bf16[384,256]{1,0:T(8,128)(2,1)} %get-tuple-element.14.din_ref, f32[64,352]{1,0:T(8,128)} %get-tuple-element.15.dg_ref, f32[64,352]{1,0:T(8,128)} %get-tuple-element.16.dv_ref, ...), custom_call_target="tpu_custom_call" | custom-call | tf_op jit(solution)/shard_map/pallas_call | solution.py:656

commit v10 on v9

--- a/solution.py
+++ b/solution.py
@@ -30,7 +30,7 @@
     "v": {8: 7, 7: 6, 6: 5, 5: 4, 4: 0, 3: 2, 2: 1, 1: 0},
 }
 ITEMS = [(h, k) for h in "gv" for k in range(ZL)]
-AHEAD, SPACING = 4, 3
+AHEAD, SPACING = 5, 3
 
 
 class Wires:
@@ -132,8 +132,6 @@
         pltpu.make_async_copy(gt_hbm, GT, local_sems.at[4]),
         pltpu.make_async_copy(vt_hbm, VT, local_sems.at[5]),
     ]
-    for load in loads:
-        load.start()
 
     barrier = pltpu.get_barrier_semaphore()
     peers = [tp_peer(k) for k in range(1, 8)]
@@ -141,6 +139,8 @@
     peers += [right, left, after, before]
     for peer in peers:
         pl.semaphore_signal(barrier, inc=1, device_id=peer, device_id_type=MESH)
+    for load in loads:
+        load.start()
     pl.semaphore_wait(barrier, len(peers))
 
     w = Wires(send_sems, recv_sems)

time: 84.4 us -> 85.5 us (1.013); the launches traced: 83.9 us -> 83.9 us
  no operation moved by 1% of the time
where the time goes in v10:
time: 85.5 us; the launch traced here: 83.9 us
  Pallas kernels  83.2 us (97%)
    pallas_call x1, Pallas kernels, shards(): pl.pallas_call(functools.partial(kernel, factor), out_shape=(tile, grad,...  81.4 us
    pallas_call x1, Pallas kernels, shards(): pl.pallas_call(finisher, out_shape=(tile, grad, grad, tap, tap), in_specs...  1.86 us

profile of v10, /device:TPU:24, one launch (start us, length us, event | category | flops | bytes accessed | tf_op | source)
XLA Modules:
  0.0 83.9 jit_solution(13040802134717945860)
XLA Ops:
  0.6 81.4 %shard_map.101 = (bf16[384,256]{1,0:T(8,128)(2,1)}, f32[64,352]{1,0:T(8,128)}, f32[64,352]{1,0:T(8,128)}, f32[8,8,352]{2,1,0:T(8,128)}) custom-call(bf16[384,256]{1,0:T(8,128)(2,1)} %bitcast.6, bf16[64,352]{1,0:T(8,128)(2,1)} %wg_hbm.1, bf16[64,352]{1,0:T(8,128)(2,1)} %wv_hbm.1, f32[3,2816]{1,0:T(4,128)} %gt_hbm.1, f32[3,2816]{1,0:T(4,128)} %vt_hbm.1, ...), custom_call_target="tpu_custom_call" | custom-call | tf_op jit(solution)/shard_map/pallas_call | solution.py:646
  82.0 1.9 %shard_map.102 = (bf16[384,256]{1,0:T(8,128)(2,1)}, f32[64,352]{1,0:T(8,128)}, f32[64,352]{1,0:T(8,128)}, f32[3,2816]{1,0:T(4,128)}, f32[3,2816]{1,0:T(4,128)}) custom-call(bf16[384,256]{1,0:T(8,128)(2,1)} %get-tuple-element.14.din_ref, f32[64,352]{1,0:T(8,128)} %get-tuple-element.15.dg_ref, f32[64,352]{1,0:T(8,128)} %get-tuple-element.16.dv_ref, ...), custom_call_target="tpu_custom_call" | custom-call | tf_op jit(solution)/shard_map/pallas_call | solution.py:656
